TPU v7x, 32 devices: a whole 2x2x4 slice. The times are simulated.
32 devices in a mesh: grp: 2 (over x), ep: 16 (over z, y, core).
Axes of the slice: x: 2, y: 2, z: 4, core: 2. Of those that a mesh axis runs over, the one named last changes fastest.
Arguments:
- tokens: bfloat16 [128, 2048], P(('grp', 'ep')), parts along dimension 0, may hold values from -6 to 6
- memory_state: float32 [128, 4, 256, 512], P(('grp', 'ep')), parts along dimension 0, may hold values from -0.6 to 0.6
- max_state: float32 [128, 4], P(('grp', 'ep')), parts along dimension 0, may hold values from -4 to 4
- norm_gain: float32 [2048], replicated, may hold values from 0.1 to 1.9
- query_weight: bfloat16 [2048, 1024], P(None, 'ep'), may hold values from -0.125 to 0.125
- key_weight: bfloat16 [2048, 1024], P(None, 'ep'), may hold values from -0.125 to 0.125
- value_weight: bfloat16 [2048, 2048], P(None, 'ep'), may hold values from -0.125 to 0.125
- output_gate: bfloat16 [2048, 2048], P(None, 'ep'), may hold values from -0.125 to 0.125
- input_gate: bfloat16 [2048, 4], replicated, may hold values from -0.125 to 0.125
- forget_gate: bfloat16 [2048, 4], replicated, may hold values from -0.125 to 0.125
- forget_bias: float32 [4], replicated, may hold values from -2 to 4
- head_gain: float32 [2048], replicated, may hold values from 0.1 to 1.9
- output_weight: bfloat16 [2048, 2048], P(None, 'ep'), may hold values from -0.125 to 0.125
- expert_norm: float32 [2048], replicated, may hold values from 0.1 to 1.9
- routed_experts: int32 [128, 4], P(('grp', 'ep')), parts along dimension 0, may hold values from 0 to 15, as said below
- route_weights: float32 [128, 4], P(('grp', 'ep')), parts along dimension 0, may hold values from 0.1 to 1
- expert_gate: bfloat16 [16, 2048, 512], P('ep'), may hold values from -0.125 to 0.125
- expert_lift: bfloat16 [16, 2048, 512], P('ep'), may hold values from -0.125 to 0.125
- expert_down: bfloat16 [16, 512, 2048], P('ep'), may hold values from -0.25 to 0.25
Outputs:
- layer_out: bfloat16 [128, 2048], P(('grp', 'ep')), parts along dimension 0
- new_memory: float32 [128, 4, 256, 512], P(('grp', 'ep')), parts along dimension 0
- new_max: float32 [128, 4], P(('grp', 'ep')), parts along dimension 0
There are 2 independent parts, one for each index of `grp`. A program takes and returns all parts, laid end to end along the dimension named above; an argument that names none is the same for every part. Nothing has to cross between parts.
Inputs may be any that keep to these rules, and one draw needn't show every extreme that they name: `routed_experts`: each row names 4 different experts of one group (expert e lies in group e // 4). No expert is named by more than 2 rows of one device, and some device has an expert named by 2 of its rows.
All inputs are finite; a program needn't handle non-finite values.
Results may differ from a plain program's by a relative error of at most 0.013.
Values may be sent and summed in bfloat16 or wider, within the bound.
A program may use at most 64 MiB of HBM per device.

v0:
```python
import functools

import jax
import jax.numpy as jnp
from jax import lax
from jax.experimental import pallas as pl
from jax.experimental.pallas import tpu as pltpu
from jax.sharding import PartitionSpec as P

epsilon = 1e-06
F32 = jnp.float32
BF16 = jnp.bfloat16
ANY = pl.BlockSpec(memory_space=pl.ANY)
VMEM = pl.BlockSpec(memory_space=pltpu.VMEM)


def scaled_norm(entries, gain):
    return entries * lax.rsqrt(jnp.mean(entries * entries, axis=-1, keepdims=True) + epsilon) * gain


def greet(n, me):
    barrier = pltpu.get_barrier_semaphore()
    for off in range(1, n):
        pl.semaphore_signal(barrier, inc=1, device_id={"ep": lax.rem(me + off, n)})
    pl.semaphore_wait(barrier, n - 1)


def exchange(n, me, source, landing, send_sem, recv_sem):
    copies = []
    for off in range(1, n):
        peer = lax.rem(me + off, n)
        copy = pltpu.make_async_remote_copy(
            src_ref=source(peer),
            dst_ref=landing.at[me],
            send_sem=send_sem.at[off],
            recv_sem=recv_sem.at[off],
            device_id={"ep": peer},
        )
        copy.start()
        copies.append(copy)
    return copies


def gather(n, me, source, landing, send_sem, recv_sem):
    partner = me + 1 - 2 * lax.rem(me, 2)

    def copy(block, origin, peer, slot):
        return pltpu.make_async_remote_copy(
            src_ref=block,
            dst_ref=landing.at[origin],
            send_sem=send_sem.at[slot],
            recv_sem=recv_sem.at[slot],
            device_id={"ep": peer},
        )

    near = [copy(source, me, partner, 1)]
    far = [copy(source, me, lax.rem(me + off, n), off) for off in range(2, n, 2)]
    for piece in far + near:
        piece.start()

    def relay():
        for off, piece in zip(range(2, n, 2), far):
            piece.wait_recv()
            origin = lax.rem(me + n - off, n)
            near.append(copy(landing.at[origin], origin, partner, off + 1))
            near[-1].start()
        finish(near)
        return far + near

    return relay


def finish(copies):
    for copy in copies:
        copy.wait_recv()


def drain(copies):
    for copy in copies:
        copy.wait_send()


def tall(table):
    return table if table.shape[1] % 128 == 0 else table.T


def across(lhs, table):
    return lax.dot_general(lhs, table, (((1,), (1,)), ((), ())), preferred_element_type=F32)


def apply(lhs, table, columns):
    if columns % 128 == 0:
        return jnp.dot(lhs, table, preferred_element_type=F32)
    return across(lhs, table)


def rows_of(ref, n):
    return jnp.concatenate([ref[j].astype(F32) for j in range(n)], axis=0)


def project_kernel(
    n, heads, key_size, value_size,
    tokens, max_state, norm_gain, wv, wg, wq, wk, w_in, w_forget, forget_bias,
    all_tokens, q_out, k_out, v_out, g_out, carried_out, written_out, max_out,
    v_s, g_s, qk_s, out_s, in_s, local_sem, send_sem, recv_sem,
):
    me = lax.axis_index("ep")
    cq, cv = q_out.shape[1] // n, v_out.shape[1] // n
    loads = [
        pltpu.make_async_copy(wv, v_s, local_sem.at[0]),
        pltpu.make_async_copy(wg, g_s, local_sem.at[1]),
        pltpu.make_async_copy(wq, qk_s.at[0], local_sem.at[2]),
        pltpu.make_async_copy(wk, qk_s.at[1], local_sem.at[3]),
    ]
    for load in loads:
        load.start()
    greet(n, me)
    relay = gather(n, me, tokens, all_tokens, send_sem.at[0], recv_sem.at[0])
    all_tokens[me] = tokens[...]
    rows = tokens.shape[0]
    gain = norm_gain[...]
    own = scaled_norm(tokens[...].astype(F32), gain).astype(BF16)
    input_logit = across(own, w_in[...])
    raw = across(own, w_forget[...]) + forget_bias[...]
    log_forget = jnp.minimum(raw, 0.0) - jnp.log1p(jnp.exp(-jnp.abs(raw)))
    prior = log_forget + max_state[...]
    new_max = jnp.maximum(prior, input_logit)
    max_out[...] = new_max
    carried_out[...] = jnp.exp(prior - new_max)
    written_out[...] = jnp.exp(input_logit - new_max) * key_size**-0.5
    for load in loads:
        load.wait()
    copies = relay()
    normed = scaled_norm(rows_of(all_tokens, n), gain).astype(BF16)
    tables = [v_s[...], g_s[...], qk_s[0], qk_s[1]]
    projected = jnp.concatenate(
        [apply(normed, table, c) for table, c in zip(tables, (cv, cv, cq, cq))], axis=1
    )
    for j in range(n):
        out_s[j] = projected[j * rows : (j + 1) * rows].astype(BF16)
    back = exchange(n, me, lambda peer: out_s.at[peer], in_s, send_sem.at[1], recv_sem.at[1])
    in_s[me] = out_s[me]
    drain(copies)
    finish(back)
    pieces = [in_s[j].astype(F32) for j in range(n)]
    v_out[...] = jnp.concatenate([b[:, :cv] for b in pieces], axis=1)
    g_out[...] = jnp.concatenate([b[:, cv : 2 * cv] for b in pieces], axis=1)
    q_out[...] = jnp.concatenate([b[:, 2 * cv : 2 * cv + cq] for b in pieces], axis=1)
    k_out[...] = jnp.concatenate([b[:, 2 * cv + cq :] for b in pieces], axis=1)
    drain(back)


def memory_kernel(
    q, k, v, g, carried, written, new_max_in, head_gain, memory,
    mixed, new_memory, max_out,
    mem_s, new_s, qt_s, kt_s, v_s, c_s, ro_s, in_sem, out_sem,
):
    rows, heads, key_size, value_size = memory.shape

    def load(h, s):
        return pltpu.make_async_copy(memory.at[s, h], mem_s.at[s, h], in_sem.at[h, s])

    def save(h, s):
        return pltpu.make_async_copy(new_s.at[s, h], new_memory.at[s, h], out_sem.at[h, s])

    for h in range(heads):
        for s in range(rows):
            load(h, s).start()
    max_out[...] = new_max_in[...]
    pad = jnp.zeros((8 - rows % 8 if rows % 8 else 0, q.shape[1]), F32)
    qt_s[...] = jnp.concatenate([q[...], pad], axis=0).T
    kt_s[...] = jnp.concatenate([k[...], pad], axis=0).T
    for h in range(heads):
        c_s[h] = jnp.broadcast_to(carried[:, h : h + 1], (rows, value_size))
        v_s[h] = v[:, h * value_size : (h + 1) * value_size] * written[:, h : h + 1]
    step = 32

    def head(h, carry):
        for s in range(rows):
            load(h, s).wait()
            keep = c_s[h, s : s + 1, :]
            values = v_s[h, s : s + 1, :]

            def chunk(r, total):
                at = pl.multiple_of(r * step, step)
                col = pl.ds(pl.multiple_of(h * key_size + at, step), step)
                new = (
                    keep * mem_s[s, h, pl.ds(at, step), :] + kt_s[col, s : s + 1] * values
                )
                new_s[s, h, pl.ds(at, step), :] = new
                terms = (qt_s[col, s : s + 1] * new).reshape(step // 8, 8, value_size)
                return total + jnp.sum(terms, axis=0)

            total = lax.fori_loop(
                0, key_size // step, chunk, jnp.zeros((8, value_size), F32), unroll=True
            )
            save(h, s).start()
            ro_s[h, s : s + 1, :] = jnp.sum(total, axis=0, keepdims=True)
        return carry

    lax.fori_loop(0, heads, head, 0)
    for h in range(heads):
        cols = slice(h * value_size, (h + 1) * value_size)
        part = scaled_norm(ro_s[h], head_gain[:, cols]) * jax.nn.sigmoid(g[:, cols])
        mixed[:, cols] = part.astype(BF16)
    for h in range(heads):
        for s in range(rows):
            save(h, s).wait()


def expert_kernel(
    n,
    mixed, all_tokens, expert_norm, routed, route_weights, w_out, w_gate, w_lift, w_down,
    layer_out,
    wo_s, wg_s, wl_s, wd_s, mix_s, col_s, cols_s, res_s, out_s, in_s, local_sem, send_sem, recv_sem,
):
    me = lax.axis_index("ep")
    rows, width = mixed.shape
    loads = [
        pltpu.make_async_copy(w_out, wo_s, local_sem.at[0]),
        pltpu.make_async_copy(w_gate.at[0], wg_s, local_sem.at[1]),
        pltpu.make_async_copy(w_lift.at[0], wl_s, local_sem.at[2]),
        pltpu.make_async_copy(w_down.at[0], wd_s, local_sem.at[3]),
    ]
    for load in loads:
        load.start()
    greet(n, me)
    relay = gather(n, me, mixed, mix_s, send_sem.at[0], recv_sem.at[0])
    mix_s[me] = mixed[...]
    loads[0].wait()
    first = relay()
    col_s[...] = apply(rows_of(mix_s, n).astype(BF16), wo_s[...], col_s.shape[1]).astype(BF16)
    relay = gather(n, me, col_s, cols_s, send_sem.at[1], recv_sem.at[1])
    cols_s[me] = col_s[...]
    inputs = rows_of(all_tokens, n)
    drain(first)
    second = relay()
    branch = jnp.concatenate([cols_s[j].astype(F32) for j in range(n)], axis=1)
    residual = (inputs + branch).astype(BF16).astype(F32)
    for j in range(n):
        res_s[j] = residual[j * rows : (j + 1) * rows]
    expert_in = scaled_norm(residual, expert_norm[...]).astype(BF16)
    for load in loads[1:]:
        load.wait()
    gate_value = jnp.dot(expert_in, wg_s[...], preferred_element_type=F32)
    lift_value = jnp.dot(expert_in, wl_s[...], preferred_element_type=F32)
    hidden = (jax.nn.silu(gate_value) * lift_value).astype(BF16)
    result = jnp.dot(hidden, wd_s[...], preferred_element_type=F32)
    for j in range(n):
        out_s[j] = result[j * rows : (j + 1) * rows].astype(BF16)
    third = exchange(n, me, lambda peer: out_s.at[peer], in_s, send_sem.at[2], recv_sem.at[2])
    in_s[me] = out_s[me]
    drain(second)
    which = routed[...]
    weights = route_weights[...]
    finish(third)
    total = jnp.zeros((rows, width), F32)
    for j in range(n):
        weight = jnp.sum(jnp.where(which == j, weights, 0.0), axis=1, keepdims=True)
        total = total + (weight * in_s[j].astype(F32)).astype(BF16).astype(F32)
    layer_out[...] = (res_s[me] + total).astype(BF16)
    drain(third)


def body(
    tokens, memory_state, max_state, norm_gain, query_weight, key_weight, value_weight,
    output_gate, input_gate, forget_gate, forget_bias, head_gain, output_weight, expert_norm,
    routed_experts, route_weights, expert_gate, expert_lift, expert_down,
):
    n = lax.axis_size("ep")
    rows, width = tokens.shape
    _, heads, key_size, value_size = memory_state.shape
    hidden = expert_gate.shape[2]
    cq, cv = query_weight.shape[1], value_weight.shape[1]
    total_cols = 2 * cq + 2 * cv
    wv, wg, wq, wk = (tall(t) for t in (value_weight, output_gate, query_weight, key_weight))
    wo = tall(output_weight)
    sds = jax.ShapeDtypeStruct
    small = sds((rows, heads), F32)
    all_tokens, q, k, v, g, carried, written, top = pl.pallas_call(
        functools.partial(project_kernel, n, heads, key_size, value_size),
        out_shape=(
            sds((n, rows, width), BF16),
            sds((rows, n * cq), F32),
            sds((rows, n * cq), F32),
            sds((rows, n * cv), F32),
            sds((rows, n * cv), F32),
            small, small, small,
        ),
        in_specs=[VMEM] * 3 + [ANY] * 4 + [VMEM] * 3,
        out_specs=[VMEM] * 8,
        scratch_shapes=[
            pltpu.VMEM(wv.shape, BF16),
            pltpu.VMEM(wg.shape, BF16),
            pltpu.VMEM((2, *wq.shape), BF16),
            pltpu.VMEM((n, rows, total_cols), BF16),
            pltpu.VMEM((n, rows, total_cols), BF16),
            pltpu.SemaphoreType.DMA((4,)),
            pltpu.SemaphoreType.DMA((2, n)),
            pltpu.SemaphoreType.DMA((2, n)),
        ],
        compiler_params=pltpu.CompilerParams(collective_id=0, has_side_effects=True),
        name="project",
    )(
        tokens, max_state, norm_gain.reshape(1, -1), wv, wg, wq, wk,
        input_gate.T, forget_gate.T, forget_bias.reshape(1, -1),
    )
    mixed, new_memory, new_max = pl.pallas_call(
        memory_kernel,
        out_shape=(sds((rows, width), BF16), sds(memory_state.shape, F32), small),
        in_specs=[VMEM] * 8 + [ANY],
        out_specs=[VMEM, ANY, VMEM],
        scratch_shapes=[
            pltpu.VMEM(memory_state.shape, F32),
            pltpu.VMEM(memory_state.shape, F32),
            pltpu.VMEM((heads * key_size, -(-rows // 8) * 8), F32),
            pltpu.VMEM((heads * key_size, -(-rows // 8) * 8), F32),
            pltpu.VMEM((heads, rows, value_size), F32),
            pltpu.VMEM((heads, rows, value_size), F32),
            pltpu.VMEM((heads, rows, value_size), F32),
            pltpu.SemaphoreType.DMA((heads, rows)),
            pltpu.SemaphoreType.DMA((heads, rows)),
        ],
        name="memory",
    )(q, k, v, g, carried, written, top, head_gain.reshape(1, -1), memory_state)
    layer_out = pl.pallas_call(
        functools.partial(expert_kernel, n),
        out_shape=sds((rows, width), BF16),
        in_specs=[VMEM] * 5 + [ANY] * 4,
        out_specs=VMEM,
        scratch_shapes=[
            pltpu.VMEM(wo.shape, BF16),
            pltpu.VMEM((width, hidden), BF16),
            pltpu.VMEM((width, hidden), BF16),
            pltpu.VMEM((hidden, width), BF16),
            pltpu.VMEM((n, rows, width), BF16),
            pltpu.VMEM((n * rows, output_weight.shape[1]), BF16),
            pltpu.VMEM((n, n * rows, output_weight.shape[1]), BF16),
            pltpu.VMEM((n, rows, width), F32),
            pltpu.VMEM((n, rows, width), BF16),
            pltpu.VMEM((n, rows, width), BF16),
            pltpu.SemaphoreType.DMA((4,)),
            pltpu.SemaphoreType.DMA((3, n)),
            pltpu.SemaphoreType.DMA((3, n)),
        ],
        compiler_params=pltpu.CompilerParams(collective_id=1, has_side_effects=True),
        name="experts",
    )(
        mixed, all_tokens, expert_norm.reshape(1, -1), routed_experts, route_weights,
        wo, expert_gate, expert_lift, expert_down,
    )
    return layer_out, new_memory, new_max


def solution(mesh):
    both = ("grp", "ep")
    return jax.shard_map(
        body,
        mesh=mesh,
        in_specs=(
            P(both, None), P(both, None, None, None), P(both, None), P(),
            P(None, "ep"), P(None, "ep"), P(None, "ep"), P(None, "ep"),
            P(), P(), P(), P(), P(None, "ep"), P(),
            P(both, None), P(both, None),
            P("ep", None, None), P("ep", None, None), P("ep", None, None),
        ),
        out_specs=(P(both, None), P(both, None, None, None), P(both, None)),
        check_vma=False,
    )
```

profile of v0, /device:TPU:0, one launch (start us, length us, event | category | flops | bytes accessed | tf_op | source)
XLA Modules:
  0.0 52.1 jit_solution(9115811062172795017)
XLA Ops:
  0.6 18.8 %project.1 = (bf16[16,4,2048]{2,1,0:T(4,128)(2,1)}, f32[4,1024]{1,0:T(4,128)}, f32[4,1024]{1,0:T(4,128)}, f32[4,2048]{1,0:T(4,128)}, f32[4,2048]{1,0:T(4,128)}, ...) custom-call(bf16[4,2048]{1,0:T(4,128)(2,1)} %tokens.1, f32[4,4]{1,0:T(4,128)} %max_state.1, f32[1,2048]{1,0:T(1,128)} %bitcast.12, ...), custom_call_target="tpu_custom_call" | custom-call | tf_op jit(solution)/shard_map/project/pallas_call | solution.py:280
  19.5 8.1 %memory.2 = (bf16[4,2048]{1,0:T(4,128)(2,1)}, f32[4,4,256,512]{3,2,1,0:T(8,128)}, f32[4,4]{1,0:T(4,128)}) custom-call(f32[4,1024]{1,0:T(4,128)} %get-tuple-element.14.q, f32[4,1024]{1,0:T(4,128)} %get-tuple-element.15.k, f32[4,2048]{1,0:T(4,128)} %get-tuple-element.16.v, f32[4,2048]{1,0:T(4,128)} %get-tuple-element.17.g, f32[4,4]{1,0:T(4,128)} %get-tuple-element.18.carried, ...), custom_call_target="tpu_custom_call" | custom-call | tf_op jit(solution)/shard_map/memory/pallas_call | solution.py:308
  27.6 23.2 %experts.1 = bf16[4,2048]{1,0:T(4,128)(2,1)} custom-call(bf16[4,2048]{1,0:T(4,128)(2,1)} %get-tuple-element.21.mixed, bf16[16,4,2048]{2,1,0:T(4,128)(2,1)} %get-tuple-element.22.all_tokens, f32[1,2048]{1,0:T(1,128)} %bitcast.14, s32[4,4]{1,0:T(4,128)} %routed.1, f32[4,4]{1,0:T(4,128)} %route_weights.1, bf16[2048,128]{1,0:T(8,128)(2,1)} %w_out.1, ...), custom_call_target="tpu_custom_call" | custom-call | tf_op jit(solution)/shard_map/experts/pallas_call | solution.py:326
  50.8 1.3 %copy.23 = bf16[4,2048]{1,0:T(4,128)(2,1)} copy(bf16[4,2048]{1,0:T(4,128)(2,1)} %experts.1) | data formatting | bytes 32768
where the time goes:
time: 52.5 us; the launch traced here: 52.1 us
  Pallas kernels  50.1 us (95%)
  local copies, waits for them, and re-layouts  1.33 us (3%)
  between operations  0.66 us (1%)
    pallas_call x1, Pallas kernels, body(): pl.pallas_call(functools.partial(expert_kernel, n), out_shape=sds((rows,...  23.2 us
    pallas_call x1, Pallas kernels, body(): pl.pallas_call(functools.partial(project_kernel, n, heads, key_size, valu...  18.8 us
    pallas_call x1, Pallas kernels, body(): pl.pallas_call(memory_kernel, out_shape=(sds((rows, width), BF16), sds(me...  8.07 us
    unnamed x1, local copies, waits for them, and re-layouts  1.33 us

commit v1 on v0

v1 whole, which is shorter than its diff:
```python
import functools

import jax
import jax.numpy as jnp
from jax import lax
from jax.experimental import pallas as pl
from jax.experimental.pallas import tpu as pltpu
from jax.sharding import PartitionSpec as P

epsilon = 1e-06
F32 = jnp.float32
BF16 = jnp.bfloat16
ANY = pl.BlockSpec(memory_space=pl.ANY)
HBM = pl.BlockSpec(memory_space=pltpu.HBM)
VMEM = pl.BlockSpec(memory_space=pltpu.VMEM)
SLOTS = 2


def scaled_norm(entries, gain):
    return entries * lax.rsqrt(jnp.mean(entries * entries, axis=-1, keepdims=True) + epsilon) * gain


def flip(me, mask):
    peer, bit = me, 1
    while bit <= mask:
        if mask & bit:
            peer = peer + bit * (1 - 2 * lax.rem(lax.div(me, bit), 2))
        bit *= 2
    return peer


def remote(source, target, sems, phase, slot, peer):
    send_sem, recv_sem = sems
    return pltpu.make_async_remote_copy(
        src_ref=source,
        dst_ref=target,
        send_sem=send_sem.at[phase, slot],
        recv_sem=recv_sem.at[phase, slot],
        device_id={"ep": peer},
    )


def exchange(n, me, source, landing, sems, phase):
    copies = []
    for mask in range(n - 1, 0, -1):
        peer = flip(me, mask)
        copies.append(remote(source(peer), landing.at[me], sems, phase, mask, peer))
        copies[-1].start()
    return copies


def gather(n, me, source, landing, sems, phase):
    partner = flip(me, 1)
    far = {m: remote(source, landing.at[me], sems, phase, m, flip(me, m)) for m in range(n - 2, 0, -2)}
    for piece in far.values():
        piece.start()
    near = [remote(source, landing.at[me], sems, phase, 1, partner)]
    near[0].start()

    def relay():
        for m in range(2, n, 2):
            far[m].wait_recv()
            origin = flip(me, m)
            near.append(remote(landing.at[origin], landing.at[origin], sems, phase, m + 1, partner))
            near[-1].start()
        finish(near)
        return list(far.values()) + near

    return relay


def finish(copies):
    for copy in copies:
        copy.wait_recv()


def drain(copies):
    for copy in copies:
        copy.wait_send()


def tall(table):
    return table if table.shape[1] % 128 == 0 else table.T


def across(lhs, table):
    return lax.dot_general(lhs, table, (((1,), (1,)), ((), ())), preferred_element_type=F32)


def apply(lhs, table, columns):
    if columns % 128 == 0:
        return jnp.dot(lhs, table, preferred_element_type=F32)
    return across(lhs, table)


def rows_of(ref, n, start, size):
    return jnp.concatenate([ref[j, :, start : start + size].astype(F32) for j in range(n)], axis=0)


def own_columns(ref, n, me, columns):
    if columns % 128 == 0:
        at = pl.ds(pl.multiple_of(me * columns, 128), columns)
        return jnp.concatenate([ref[j, :, at].astype(F32) for j in range(n)], axis=0)
    share = 128 // columns
    at = pl.ds(pl.multiple_of(lax.div(me, share) * 128, 128), 128)
    wide = jnp.concatenate([ref[j, :, at].astype(F32) for j in range(n)], axis=0)
    part = lax.rem(me, share)
    picked = wide[:, :columns]
    for i in range(1, share):
        picked = jnp.where(part == i, wide[:, i * columns : (i + 1) * columns], picked)
    return picked


def layer_kernel(
    n, heads, key_size, value_size, names_width,
    tokens, memory, max_state, norm_gain, wv, wg, wq, wk, w_in, w_forget, forget_bias,
    head_gain, wo, expert_norm, routed, route_weights, w_gate, w_lift, w_down,
    new_memory, results, residual_out, picks_out, max_out,
    tok_s, max_s, ngain_s, v_w, g_w, q_w, k_w, in_w, forget_w, bias_s,
    hgain_s, o_w, egain_s, routed_s, rw_s, gate_w, lift_w, down_w,
    all_s, names_s, pick_s, x_s, proj_s, back_s, qt_s, kt_s, v_s, c_s, ro_s, mix_s,
    res_s, needed_s, own_s, owned_s, out_s,
    local_sem, mem_sem, send_sem, recv_sem,
):
    me = lax.axis_index("ep")
    barrier = pltpu.get_barrier_semaphore()
    for mask in range(n - 1, 0, -1):
        pl.semaphore_signal(barrier, inc=1, device_id={"ep": flip(me, mask)})
    rows, width = tokens.shape
    sems = (send_sem, recv_sem)
    pairs = [
        (tokens, tok_s.at[:, pl.ds(0, width)]), (routed, routed_s), (norm_gain, ngain_s),
        (w_in, in_w), (w_forget, forget_w), (forget_bias, bias_s), (max_state, max_s),
        (route_weights, rw_s), (wv, v_w), (wg, g_w), (wq, q_w), (wk, k_w),
        (head_gain, hgain_s), (expert_norm, egain_s), (wo, o_w),
        (w_gate.at[0], gate_w), (w_lift.at[0], lift_w), (w_down.at[0], down_w),
    ]
    loads = [pltpu.make_async_copy(a, b, local_sem.at[i]) for i, (a, b) in enumerate(pairs)]
    for load in loads[:12]:
        load.start()

    def fetch(h, s):
        return pltpu.make_async_copy(memory.at[s, h], new_memory.at[s, h], mem_sem.at[h, s])

    for h in range(heads):
        for s in range(rows):
            fetch(h, s).start()
    for load in loads[12:]:
        load.start()

    for load in loads[:8]:
        load.wait()
    lane = lax.broadcasted_iota(jnp.int32, (rows, names_width), 1)
    which = routed_s[...]
    weights = rw_s[...]
    taken = jnp.zeros((1, names_width), F32)
    chosen = []
    named = jnp.zeros((rows, names_width), F32)
    weighed = jnp.zeros((rows, names_width), F32)
    for slot in range(SLOTS):
        for k in range(which.shape[1]):
            hit = lane == which[:, k : k + 1] + slot * n
            named = named + hit.astype(F32)
            weighed = weighed + jnp.where(hit, weights[:, k : k + 1], 0.0)
    slot_of = (lax.broadcasted_iota(jnp.int32, (1, names_width), 1) >= n).astype(F32)
    for r in range(rows):
        chosen.append(named[r : r + 1] * (taken == slot_of).astype(F32))
        taken = taken + named[r : r + 1]
    chosen = jnp.concatenate(chosen, axis=0)
    tok_s[:, width:] = chosen.astype(BF16)
    picks_out[...] = chosen * weighed

    gain = ngain_s[...]
    own = scaled_norm(tok_s[:, :width].astype(F32), gain).astype(BF16)
    input_logit = across(own, in_w[...])
    raw = across(own, forget_w[...]) + bias_s[...]
    log_forget = jnp.minimum(raw, 0.0) - jnp.log1p(jnp.exp(-jnp.abs(raw)))
    prior = log_forget + max_s[...]
    new_max = jnp.maximum(prior, input_logit)
    max_out[...] = new_max
    carried = jnp.exp(prior - new_max)
    written = jnp.exp(input_logit - new_max) * key_size**-0.5

    pl.semaphore_wait(barrier, n - 1)
    relay = gather(n, me, tok_s, all_s, sems, 0)
    all_s[me] = tok_s[...]
    for load in loads[8:12]:
        load.wait()
    sent = relay()
    normed = scaled_norm(rows_of(all_s, n, 0, width), gain).astype(BF16)
    cq, cv = heads * key_size // n, heads * value_size // n
    tables = [v_w[...], g_w[...], q_w[...], k_w[...]]
    projected = jnp.concatenate(
        [apply(normed, table, c) for table, c in zip(tables, (cv, cv, cq, cq))], axis=1
    )
    for j in range(n):
        proj_s[j] = projected[j * rows : (j + 1) * rows].astype(BF16)
    back = exchange(n, me, lambda peer: proj_s.at[peer], back_s, sems, 1)
    back_s[me] = proj_s[me]

    columns = res_s.shape[1]
    x_s[...] = own_columns(all_s, n, me, columns)
    names_s[...] = rows_of(all_s, n, width, names_width).T
    wanted = SLOTS * n
    place = lax.broadcasted_iota(jnp.int32, (wanted, n * rows), 0)
    row = lax.broadcasted_iota(jnp.int32, (wanted, n * rows), 1)
    first = (place - place % SLOTS) // SLOTS * rows
    inside = (row >= first) & (row < first + rows)
    even = place % SLOTS == 0
    for j in range(n):
        value = jnp.where(even, names_s[j : j + 1, :], names_s[n + j : n + j + 1, :])
        pick_s[j] = jnp.where(inside, value, 0.0).astype(BF16)
    loads[12].wait()
    loads[13].wait()
    loads[14].wait()
    for h in range(heads):
        for s in range(rows):
            fetch(h, s).wait()
    finish(back)

    pieces = [back_s[j].astype(F32) for j in range(n)]
    v = jnp.concatenate([b[:, :cv] for b in pieces], axis=1)
    g = jnp.concatenate([b[:, cv : 2 * cv] for b in pieces], axis=1)
    q = jnp.concatenate([b[:, 2 * cv : 2 * cv + cq] for b in pieces], axis=1)
    k = jnp.concatenate([b[:, 2 * cv + cq :] for b in pieces], axis=1)
    pad = jnp.zeros((-rows % 8, q.shape[1]), F32)
    qt_s[...] = jnp.concatenate([q, pad], axis=0).T
    kt_s[...] = jnp.concatenate([k, pad], axis=0).T
    for h in range(heads):
        c_s[h] = jnp.broadcast_to(carried[:, h : h + 1], (rows, value_size))
        v_s[h] = v[:, h * value_size : (h + 1) * value_size] * written[:, h : h + 1]
    step = 32

    def read(h, carry):
        for s in range(rows):

            def chunk(r, total):
                at = pl.multiple_of(r * step, step)
                col = pl.ds(pl.multiple_of(h * key_size + at, step), step)
                terms = qt_s[col, s : s + 1] * new_memory[s, h, pl.ds(at, step), :]
                return total + jnp.sum(terms.reshape(step // 8, 8, value_size), axis=0)

            total = lax.fori_loop(
                0, key_size // step, chunk, jnp.zeros((8, value_size), F32), unroll=True
            )
            ro_s[h, s : s + 1, :] = jnp.sum(total, axis=0, keepdims=True)
        return carry

    lax.fori_loop(0, heads, read, 0)
    for h in range(heads):
        cols = slice(h * value_size, (h + 1) * value_size)
        keys = slice(h * key_size, (h + 1) * key_size)
        match = jnp.sum(q[:, keys] * k[:, keys], axis=1, keepdims=True)
        readout = c_s[h] * ro_s[h] + match * v_s[h]
        part = scaled_norm(readout, hgain_s[:, cols]) * jax.nn.sigmoid(g[:, cols])
        mix_s[me, :, cols] = part.astype(BF16)
    relay = gather(n, me, mix_s.at[me], mix_s, sems, 2)

    def update(h, carry):
        for s in range(rows):
            keep = c_s[h, s : s + 1, :]
            values = v_s[h, s : s + 1, :]

            def chunk(r, nothing):
                at = pl.multiple_of(r * step, step)
                col = pl.ds(pl.multiple_of(h * key_size + at, step), step)
                new_memory[s, h, pl.ds(at, step), :] = (
                    keep * new_memory[s, h, pl.ds(at, step), :] + kt_s[col, s : s + 1] * values
                )
                return nothing

            lax.fori_loop(0, key_size // step, chunk, 0, unroll=True)
        return carry

    lax.fori_loop(0, heads, update, 0)
    sent += relay()
    branch = apply(rows_of(mix_s, n, 0, width).astype(BF16), o_w[...], columns).astype(BF16)
    residual = (x_s[...] + branch.astype(F32)).astype(BF16)
    picked = jnp.dot(
        pick_s[...].reshape(n * wanted, n * rows), residual, preferred_element_type=F32
    ).astype(BF16)
    res_s[...] = picked
    there = exchange(
        n, me, lambda peer: res_s.at[pl.ds(pl.multiple_of(peer * wanted, wanted), wanted)],
        needed_s, sems, 3,
    )
    needed_s[me] = res_s[pl.ds(pl.multiple_of(me * wanted, wanted), wanted)]
    whole = residual.astype(F32)
    for j in range(n):
        own_s[j] = whole[j * rows : (j + 1) * rows].astype(BF16)
    home = exchange(n, me, lambda peer: own_s.at[peer], owned_s, sems, 4)
    owned_s[me] = own_s[me]
    for load in loads[15:]:
        load.wait()
    finish(there)
    needed = jnp.concatenate([needed_s[j].astype(F32) for j in range(n)], axis=1)
    expert_in = scaled_norm(needed, egain_s[...]).astype(BF16)
    gate_value = jnp.dot(expert_in, gate_w[...], preferred_element_type=F32)
    lift_value = jnp.dot(expert_in, lift_w[...], preferred_element_type=F32)
    hidden = (jax.nn.silu(gate_value) * lift_value).astype(BF16)
    result = jnp.dot(hidden, down_w[...], preferred_element_type=F32)
    for j in range(n):
        out_s[j] = result[j * SLOTS : (j + 1) * SLOTS].astype(BF16)
    last = exchange(n, me, lambda peer: out_s.at[peer], results, sems, 5)
    results[me] = out_s[me]
    finish(home)
    residual_out[...] = jnp.concatenate([owned_s[j].astype(F32) for j in range(n)], axis=1)
    drain(sent + back + there + home)
    finish(last)
    drain(last)


def combine_kernel(
    memory, results, residual, picks, new_max_in,
    layer_out, new_memory, max_out,
    out_s, top_s, mem_sem, sem,
):
    n, slots, width = results.shape
    rows, heads = new_max_in.shape

    def save(h, s):
        return pltpu.make_async_copy(memory.at[s, h], new_memory.at[s, h], mem_sem.at[h, s])

    for h in range(heads):
        for s in range(rows):
            save(h, s).start()
    top_s[...] = new_max_in[...]
    top = pltpu.make_async_copy(top_s, max_out, sem.at[0])
    top.start()
    weights = picks[...]
    total = jnp.zeros((rows, width), F32)
    for j in range(n):
        block = results[j].astype(F32)
        for s in range(slots):
            weight = weights[:, s * n + j : s * n + j + 1]
            total = total + (weight * block[s : s + 1]).astype(BF16).astype(F32)
    out_s[...] = (residual[...] + total).astype(BF16)
    out = pltpu.make_async_copy(out_s, layer_out, sem.at[1])
    out.start()
    for h in range(heads):
        for s in range(rows):
            save(h, s).wait()
    top.wait()
    out.wait()


def body(
    tokens, memory_state, max_state, norm_gain, query_weight, key_weight, value_weight,
    output_gate, input_gate, forget_gate, forget_bias, head_gain, output_weight, expert_norm,
    routed_experts, route_weights, expert_gate, expert_lift, expert_down,
):
    n = lax.axis_size("ep")
    rows, width = tokens.shape
    _, heads, key_size, value_size = memory_state.shape
    hidden = expert_gate.shape[2]
    cq, cv, columns = query_weight.shape[1], value_weight.shape[1], output_weight.shape[1]
    total_cols = 2 * cq + 2 * cv
    wv, wg, wq, wk = (tall(t) for t in (value_weight, output_gate, query_weight, key_weight))
    wo = tall(output_weight)
    names_width = -(-SLOTS * n // 128) * 128
    wanted = SLOTS * n
    sds = jax.ShapeDtypeStruct
    small = sds((rows, heads), F32)
    padded = -(-rows // 8) * 8
    new_memory, results, residual, picks, new_max = pl.pallas_call(
        functools.partial(layer_kernel, n, heads, key_size, value_size, names_width),
        out_shape=(
            pltpu.VMEM(memory_state.shape, F32),
            pltpu.VMEM((n, SLOTS, width), BF16),
            pltpu.VMEM((rows, width), F32),
            pltpu.VMEM((rows, names_width), F32),
            pltpu.VMEM((rows, heads), F32),
        ),
        in_specs=[HBM] * 19,
        out_specs=[VMEM] * 5,
        scratch_shapes=[
            pltpu.VMEM((rows, width + names_width), BF16),
            pltpu.VMEM((rows, heads), F32),
            pltpu.VMEM((1, width), F32),
            pltpu.VMEM(wv.shape, BF16),
            pltpu.VMEM(wg.shape, BF16),
            pltpu.VMEM(wq.shape, BF16),
            pltpu.VMEM(wk.shape, BF16),
            pltpu.VMEM((heads, width), BF16),
            pltpu.VMEM((heads, width), BF16),
            pltpu.VMEM((1, heads), F32),
            pltpu.VMEM((1, width), F32),
            pltpu.VMEM(wo.shape, BF16),
            pltpu.VMEM((1, width), F32),
            pltpu.VMEM(routed_experts.shape, jnp.int32),
            pltpu.VMEM(route_weights.shape, F32),
            pltpu.VMEM((width, hidden), BF16),
            pltpu.VMEM((width, hidden), BF16),
            pltpu.VMEM((hidden, width), BF16),
            pltpu.VMEM((n, rows, width + names_width), BF16),
            pltpu.VMEM((names_width, n * rows), F32),
            pltpu.VMEM((n, wanted, n * rows), BF16),
            pltpu.VMEM((n * rows, columns), F32),
            pltpu.VMEM((n, rows, total_cols), BF16),
            pltpu.VMEM((n, rows, total_cols), BF16),
            pltpu.VMEM((heads * key_size, padded), F32),
            pltpu.VMEM((heads * key_size, padded), F32),
            pltpu.VMEM((heads, rows, value_size), F32),
            pltpu.VMEM((heads, rows, value_size), F32),
            pltpu.VMEM((heads, rows, value_size), F32),
            pltpu.VMEM((n, rows, width), BF16),
            pltpu.VMEM((n * wanted, columns), BF16),
            pltpu.VMEM((n, wanted, columns), BF16),
            pltpu.VMEM((n, rows, columns), BF16),
            pltpu.VMEM((n, rows, columns), BF16),
            pltpu.VMEM((n, SLOTS, width), BF16),
            pltpu.SemaphoreType.DMA((18,)),
            pltpu.SemaphoreType.DMA((heads, rows)),
            pltpu.SemaphoreType.DMA((6, n)),
            pltpu.SemaphoreType.DMA((6, n)),
        ],
        compiler_params=pltpu.CompilerParams(
            collective_id=0, has_side_effects=True, vmem_limit_bytes=40 << 20
        ),
        name="layer",
    )(*(
        pltpu.with_memory_space_constraint(x, pltpu.HBM)
        for x in (
            tokens, memory_state, max_state, norm_gain.reshape(1, -1), wv, wg, wq, wk,
            input_gate.T, forget_gate.T, forget_bias.reshape(1, -1), head_gain.reshape(1, -1), wo,
            expert_norm.reshape(1, -1), routed_experts, route_weights,
            expert_gate, expert_lift, expert_down,
        )
    ))
    layer_out, new_memory, new_max = pl.pallas_call(
        combine_kernel,
        out_shape=(sds((rows, width), BF16), sds(memory_state.shape, F32), small),
        in_specs=[VMEM] * 5,
        out_specs=[ANY] * 3,
        scratch_shapes=[
            pltpu.VMEM((rows, width), BF16),
            pltpu.VMEM((rows, heads), F32),
            pltpu.SemaphoreType.DMA((heads, rows)),
            pltpu.SemaphoreType.DMA((2,)),
        ],
        compiler_params=pltpu.CompilerParams(vmem_limit_bytes=8 << 20),
        name="combine",
    )(new_memory, results, residual, picks, new_max)
    return layer_out, new_memory, new_max


def solution(mesh):
    both = ("grp", "ep")
    return jax.shard_map(
        body,
        mesh=mesh,
        in_specs=(
            P(both, None), P(both, None, None, None), P(both, None), P(),
            P(None, "ep"), P(None, "ep"), P(None, "ep"), P(None, "ep"),
            P(), P(), P(), P(), P(None, "ep"), P(),
            P(both, None), P(both, None),
            P("ep", None, None), P("ep", None, None), P("ep", None, None),
        ),
        out_specs=(P(both, None), P(both, None, None, None), P(both, None)),
        check_vma=False,
    )
```

time: 52.5 us -> 41.6 us (0.79)
  Pallas kernels: 50.1 us -> 40.7 us
  local copies, waits for them, and re-layouts: 1.33 us -> 0 us
    pallas_call x3 -> x2, Pallas kernels: 50.1 us -> 40.7 us  [the longest x1 37.3 us: body(): pl.pallas_call(functools.partial(layer_kernel, n, heads, key_size, value_...]
    unnamed x1 -> x0, local copies, waits for them, and re-layouts: 1.33 us -> none
where the time goes in v1:
time: 41.6 us; the launch traced here: 41.4 us
  Pallas kernels  40.7 us (98%)
  between operations  0.65 us (2%)
    pallas_call x1, Pallas kernels, body(): pl.pallas_call(functools.partial(layer_kernel, n, heads, key_size, value_...  37.3 us
    pallas_call x1, Pallas kernels, body(): pl.pallas_call(combine_kernel, out_shape=(sds((rows, width), BF16), sds(m...  3.45 us

profile of v1, /device:TPU:0, one launch (start us, length us, event | category | flops | bytes accessed | tf_op | source)
XLA Modules:
  0.0 41.4 jit_solution(18130339726422058418)
XLA Ops:
  0.6 37.3 %layer.1 = (f32[4,4,256,512]{3,2,1,0:T(8,128)S(1)}, bf16[16,2,2048]{2,1,0:T(2,128)(2,1)S(1)}, f32[4,2048]{1,0:T(4,128)S(1)}, f32[4,128]{1,0:T(4,128)S(1)}, f32[4,4]{1,0:T(4,128)S(1)}) custom-call(bf16[4,2048]{1,0:T(4,128)(2,1)} %tokens.1, f32[4,4,256,512]{3,2,1,0:T(8,128)} %memory.1, f32[4,4]{1,0:T(4,128)} %max_state.1, f32[1,2048]{1,0:T(1,128)} %bitcast.12, ...), custom_call_target="tpu_custom_call" | custom-call | tf_op jit(solution)/shard_map/layer/pallas_call | solution.py:365
  37.9 3.5 %combine.1 = (bf16[4,2048]{1,0:T(4,128)(2,1)}, f32[4,4,256,512]{3,2,1,0:T(8,128)}, f32[4,4]{1,0:T(4,128)}) custom-call(f32[4,4,256,512]{3,2,1,0:T(8,128)S(1)} %get-tuple-element.8.memory, bf16[16,2,2048]{2,1,0:T(2,128)(2,1)S(1)} %get-tuple-element.9.results, f32[4,2048]{1,0:T(4,128)S(1)} %get-tuple-element.10.residual, ...), custom_call_target="tpu_custom_call" | custom-call | tf_op jit(solution)/shard_map/combine/pallas_call | solution.py:430

commit v2 on v1

--- a/solution.py
+++ b/solution.py
@@ -29,54 +29,39 @@
     return peer
 
 
-def remote(source, target, sems, phase, slot, peer):
-    send_sem, recv_sem = sems
+def remote(source, target, send_sem, recv_sem, peer):
     return pltpu.make_async_remote_copy(
-        src_ref=source,
-        dst_ref=target,
-        send_sem=send_sem.at[phase, slot],
-        recv_sem=recv_sem.at[phase, slot],
-        device_id={"ep": peer},
-    )
-
-
-def exchange(n, me, source, landing, sems, phase):
-    copies = []
+        src_ref=source, dst_ref=target, send_sem=send_sem, recv_sem=recv_sem, device_id={"ep": peer}
+    )
+
+
+def exchange(n, me, source, landing, send_sem, recv_sem):
     for mask in range(n - 1, 0, -1):
         peer = flip(me, mask)
-        copies.append(remote(source(peer), landing.at[me], sems, phase, mask, peer))
-        copies[-1].start()
-    return copies
-
-
-def gather(n, me, source, landing, sems, phase):
+        remote(source(peer), landing.at[me], send_sem, recv_sem(mask), peer).start()
+
+
+def spread(n, me, source, target, send_sem, far_sem, near_sem):
+    for mask in [*range(n - 2, 0, -2), 1]:
+        sem = near_sem if mask == 1 else far_sem.at[mask // 2]
+        remote(source, target, send_sem, sem, flip(me, mask)).start()
+
+
+def relay(n, me, block_of, send_sem, far_sem, near_sem):
     partner = flip(me, 1)
-    far = {m: remote(source, landing.at[me], sems, phase, m, flip(me, m)) for m in range(n - 2, 0, -2)}
-    for piece in far.values():
-        piece.start()
-    near = [remote(source, landing.at[me], sems, phase, 1, partner)]
-    near[0].start()
-
-    def relay():
-        for m in range(2, n, 2):
-            far[m].wait_recv()
-            origin = flip(me, m)
-            near.append(remote(landing.at[origin], landing.at[origin], sems, phase, m + 1, partner))
-            near[-1].start()
-        finish(near)
-        return list(far.values()) + near
-
-    return relay
-
-
-def finish(copies):
-    for copy in copies:
-        copy.wait_recv()
-
-
-def drain(copies):
-    for copy in copies:
-        copy.wait_send()
+    for mask in range(2, n, 2):
+        block = block_of(mask)
+        piece = remote(block, block, send_sem, far_sem.at[mask // 2], partner)
+        piece.wait_recv()
+        remote(block, block, send_sem, near_sem, partner).start()
+
+
+def arrived(blocks, sem):
+    remote(blocks, blocks, sem, sem, 0).wait_recv()
+
+
+def departed(blocks, sem):
+    remote(blocks, blocks, sem, sem, 0).wait_send()
 
 
 def tall(table):
@@ -118,16 +103,16 @@
     new_memory, results, residual_out, picks_out, max_out,
     tok_s, max_s, ngain_s, v_w, g_w, q_w, k_w, in_w, forget_w, bias_s,
     hgain_s, o_w, egain_s, routed_s, rw_s, gate_w, lift_w, down_w,
-    all_s, names_s, pick_s, x_s, proj_s, back_s, qt_s, kt_s, v_s, c_s, ro_s, mix_s,
+    all_s, names_s, pick_s, x_s, proj_s, back_s, k_s, kt_s, v_s, c_s, w_s, mix_s,
     res_s, needed_s, own_s, owned_s, out_s,
-    local_sem, mem_sem, send_sem, recv_sem,
+    local_sem, mem_sem, send_sem, far_sem, near_sem, column_sem, part_sem, group_sem,
 ):
     me = lax.axis_index("ep")
     barrier = pltpu.get_barrier_semaphore()
     for mask in range(n - 1, 0, -1):
         pl.semaphore_signal(barrier, inc=1, device_id={"ep": flip(me, mask)})
     rows, width = tokens.shape
-    sems = (send_sem, recv_sem)
+    most = pl.ds(0, n - 1)
     pairs = [
         (tokens, tok_s.at[:, pl.ds(0, width)]), (routed, routed_s), (norm_gain, ngain_s),
         (w_in, in_w), (w_forget, forget_w), (forget_bias, bias_s), (max_state, max_s),
@@ -139,12 +124,9 @@
     for load in loads[:12]:
         load.start()
 
-    def fetch(h, s):
-        return pltpu.make_async_copy(memory.at[s, h], new_memory.at[s, h], mem_sem.at[h, s])
-
     for h in range(heads):
         for s in range(rows):
-            fetch(h, s).start()
+            pltpu.make_async_copy(memory.at[s, h], new_memory.at[s, h], mem_sem).start()
     for load in loads[12:]:
         load.start()
 
@@ -182,11 +164,14 @@
     written = jnp.exp(input_logit - new_max) * key_size**-0.5
 
     pl.semaphore_wait(barrier, n - 1)
-    relay = gather(n, me, tok_s, all_s, sems, 0)
+    spread(n, me, tok_s, all_s.at[me], send_sem.at[0], far_sem.at[0], near_sem.at[0])
     all_s[me] = tok_s[...]
     for load in loads[8:12]:
         load.wait()
-    sent = relay()
+    relay(
+        n, me, lambda mask: all_s.at[flip(me, mask)], send_sem.at[0], far_sem.at[0], near_sem.at[0]
+    )
+    arrived(all_s.at[pl.ds(0, n // 2)], near_sem.at[0])
     normed = scaled_norm(rows_of(all_s, n, 0, width), gain).astype(BF16)
     cq, cv = heads * key_size // n, heads * value_size // n
     tables = [v_w[...], g_w[...], q_w[...], k_w[...]]
@@ -195,7 +180,11 @@
     )
     for j in range(n):
         proj_s[j] = projected[j * rows : (j + 1) * rows].astype(BF16)
-    back = exchange(n, me, lambda peer: proj_s.at[peer], back_s, sems, 1)
+    per = n // heads
+    exchange(
+        n, me, lambda peer: proj_s.at[peer], back_s, send_sem.at[1],
+        lambda mask: column_sem.at[mask // per],
+    )
     back_s[me] = proj_s[me]
 
     columns = res_s.shape[1]
@@ -210,51 +199,47 @@
     for j in range(n):
         value = jnp.where(even, names_s[j : j + 1, :], names_s[n + j : n + j + 1, :])
         pick_s[j] = jnp.where(inside, value, 0.0).astype(BF16)
-    loads[12].wait()
-    loads[13].wait()
-    loads[14].wait()
-    for h in range(heads):
-        for s in range(rows):
-            fetch(h, s).wait()
-    finish(back)
-
-    pieces = [back_s[j].astype(F32) for j in range(n)]
-    v = jnp.concatenate([b[:, :cv] for b in pieces], axis=1)
-    g = jnp.concatenate([b[:, cv : 2 * cv] for b in pieces], axis=1)
-    q = jnp.concatenate([b[:, 2 * cv : 2 * cv + cq] for b in pieces], axis=1)
-    k = jnp.concatenate([b[:, 2 * cv + cq :] for b in pieces], axis=1)
-    pad = jnp.zeros((-rows % 8, q.shape[1]), F32)
-    qt_s[...] = jnp.concatenate([q, pad], axis=0).T
-    kt_s[...] = jnp.concatenate([k, pad], axis=0).T
+    for load in loads[12:15]:
+        load.wait()
+    pltpu.make_async_copy(memory, new_memory, mem_sem).wait()
     for h in range(heads):
         c_s[h] = jnp.broadcast_to(carried[:, h : h + 1], (rows, value_size))
-        v_s[h] = v[:, h * value_size : (h + 1) * value_size] * written[:, h : h + 1]
+        w_s[h] = jnp.broadcast_to(written[:, h : h + 1], (rows, value_size))
     step = 32
-
-    def read(h, carry):
+    quarter = lax.div(me, per)
+    pad = jnp.zeros((-rows % 8, key_size), F32)
+
+    def read(h):
+        pieces = [back_s[h * per + t].astype(F32) for t in range(per)]
+        v = jnp.concatenate([b[:, :cv] for b in pieces], axis=1)
+        g = jnp.concatenate([b[:, cv : 2 * cv] for b in pieces], axis=1)
+        q = jnp.concatenate([b[:, 2 * cv : 2 * cv + cq] for b in pieces], axis=1)
+        k = jnp.concatenate([b[:, 2 * cv + cq :] for b in pieces], axis=1)
+        query = jnp.concatenate([q, pad], axis=0).T
+        v = v * w_s[h]
+        match = jnp.sum(q * k, axis=1, keepdims=True) * v
+        gains = hgain_s[:, pl.ds(pl.multiple_of(h * value_size, value_size), value_size)]
+        gains = gains * jax.nn.sigmoid(g)
+        sums = []
         for s in range(rows):
-
-            def chunk(r, total):
-                at = pl.multiple_of(r * step, step)
-                col = pl.ds(pl.multiple_of(h * key_size + at, step), step)
-                terms = qt_s[col, s : s + 1] * new_memory[s, h, pl.ds(at, step), :]
-                return total + jnp.sum(terms.reshape(step // 8, 8, value_size), axis=0)
-
-            total = lax.fori_loop(
-                0, key_size // step, chunk, jnp.zeros((8, value_size), F32), unroll=True
-            )
-            ro_s[h, s : s + 1, :] = jnp.sum(total, axis=0, keepdims=True)
-        return carry
-
-    lax.fori_loop(0, heads, read, 0)
-    for h in range(heads):
-        cols = slice(h * value_size, (h + 1) * value_size)
-        keys = slice(h * key_size, (h + 1) * key_size)
-        match = jnp.sum(q[:, keys] * k[:, keys], axis=1, keepdims=True)
-        readout = c_s[h] * ro_s[h] + match * v_s[h]
-        part = scaled_norm(readout, hgain_s[:, cols]) * jax.nn.sigmoid(g[:, cols])
-        mix_s[me, :, cols] = part.astype(BF16)
-    relay = gather(n, me, mix_s.at[me], mix_s, sems, 2)
+            total = jnp.zeros((8, value_size), F32)
+            for at in range(0, key_size, step):
+                terms = query[at : at + step, s : s + 1] * new_memory[s, h, at : at + step, :]
+                total = total + jnp.sum(terms.reshape(step // 8, 8, value_size), axis=0)
+            sums.append(jnp.sum(total, axis=0, keepdims=True))
+        readout = c_s[h] * jnp.concatenate(sums, axis=0) + match
+        return scaled_norm(readout, gains).astype(BF16), k, v
+
+    for i in range(heads):
+        arrived(back_s.at[pl.ds(0, per if i else per - 1)], column_sem.at[i])
+        h = flip(quarter, i)
+        mix_s[h, me], k_s[h], v_s[h] = read(h)
+        mine = mix_s.at[h, me]
+        if i < heads - 1:
+            spread(n, me, mine, mine, send_sem.at[2 + i], far_sem.at[1 + i], near_sem.at[1 + i])
+        else:
+            for mask in range(n - 1, 0, -1):
+                remote(mine, mine, send_sem.at[2 + i], group_sem.at[0], flip(me, mask)).start()
 
     def update(h, carry):
         for s in range(rows):
@@ -262,52 +247,88 @@
             values = v_s[h, s : s + 1, :]
 
             def chunk(r, nothing):
-                at = pl.multiple_of(r * step, step)
-                col = pl.ds(pl.multiple_of(h * key_size + at, step), step)
-                new_memory[s, h, pl.ds(at, step), :] = (
-                    keep * new_memory[s, h, pl.ds(at, step), :] + kt_s[col, s : s + 1] * values
+                at = pl.ds(pl.multiple_of(r * step, step), step)
+                new_memory[s, h, at, :] = (
+                    keep * new_memory[s, h, at, :] + kt_s[h, at, s : s + 1] * values
                 )
                 return nothing
 
             lax.fori_loop(0, key_size // step, chunk, 0, unroll=True)
         return carry
 
+    for h in range(heads):
+        kt_s[h] = jnp.concatenate([k_s[h], pad], axis=0).T
     lax.fori_loop(0, heads, update, 0)
-    sent += relay()
-    branch = apply(rows_of(mix_s, n, 0, width).astype(BF16), o_w[...], columns).astype(BF16)
+    for i in range(heads - 1):
+        relay(
+            n, me, lambda mask: mix_s.at[flip(quarter, mask // per ^ i), flip(me, mask)],
+            send_sem.at[2 + i], far_sem.at[1 + i], near_sem.at[1 + i],
+        )
+    for i in range(heads - 1):
+        arrived(mix_s.at[0, pl.ds(0, n // 2)], near_sem.at[1 + i])
+    arrived(mix_s.at[0, most], group_sem.at[0])
+    mixed = jnp.concatenate(
+        [
+            jnp.concatenate([mix_s[h, j].astype(F32) for j in range(n)], axis=0).astype(BF16)
+            for h in range(heads)
+        ],
+        axis=1,
+    )
+    branch = apply(mixed, o_w[...], columns).astype(BF16)
     residual = (x_s[...] + branch.astype(F32)).astype(BF16)
     picked = jnp.dot(
         pick_s[...].reshape(n * wanted, n * rows), residual, preferred_element_type=F32
     ).astype(BF16)
     res_s[...] = picked
-    there = exchange(
+    exchange(
         n, me, lambda peer: res_s.at[pl.ds(pl.multiple_of(peer * wanted, wanted), wanted)],
-        needed_s, sems, 3,
+        needed_s, send_sem.at[2 + heads], lambda mask: part_sem.at[mask // per],
     )
     needed_s[me] = res_s[pl.ds(pl.multiple_of(me * wanted, wanted), wanted)]
     whole = residual.astype(F32)
     for j in range(n):
         own_s[j] = whole[j * rows : (j + 1) * rows].astype(BF16)
-    home = exchange(n, me, lambda peer: own_s.at[peer], owned_s, sems, 4)
+    exchange(
+        n, me, lambda peer: own_s.at[peer], owned_s, send_sem.at[3 + heads],
+        lambda mask: group_sem.at[1],
+    )
     owned_s[me] = own_s[me]
     for load in loads[15:]:
         load.wait()
-    finish(there)
-    needed = jnp.concatenate([needed_s[j].astype(F32) for j in range(n)], axis=1)
-    expert_in = scaled_norm(needed, egain_s[...]).astype(BF16)
-    gate_value = jnp.dot(expert_in, gate_w[...], preferred_element_type=F32)
-    lift_value = jnp.dot(expert_in, lift_w[...], preferred_element_type=F32)
+    span = per * columns
+    gate_value = jnp.zeros((wanted, gate_w.shape[1]), F32)
+    lift_value = jnp.zeros((wanted, lift_w.shape[1]), F32)
+    square = jnp.zeros((wanted, 1), F32)
+    for i in range(heads):
+        arrived(needed_s.at[pl.ds(0, per if i else per - 1)], part_sem.at[i])
+        part = flip(quarter, i)
+        block = jnp.concatenate([needed_s[part * per + t].astype(F32) for t in range(per)], axis=1)
+        at = pl.ds(pl.multiple_of(part * span, span), span)
+        square += jnp.sum(block * block, axis=1, keepdims=True)
+        block = (block * egain_s[:, at]).astype(BF16)
+        gate_value += jnp.dot(block, gate_w[at, :], preferred_element_type=F32)
+        lift_value += jnp.dot(block, lift_w[at, :], preferred_element_type=F32)
+    scale = lax.rsqrt(square / width + epsilon)
+    gate_value, lift_value = gate_value * scale, lift_value * scale
     hidden = (jax.nn.silu(gate_value) * lift_value).astype(BF16)
     result = jnp.dot(hidden, down_w[...], preferred_element_type=F32)
     for j in range(n):
         out_s[j] = result[j * SLOTS : (j + 1) * SLOTS].astype(BF16)
-    last = exchange(n, me, lambda peer: out_s.at[peer], results, sems, 5)
+    exchange(
+        n, me, lambda peer: out_s.at[peer], results, send_sem.at[4 + heads],
+        lambda mask: group_sem.at[2],
+    )
     results[me] = out_s[me]
-    finish(home)
+    arrived(owned_s.at[most], group_sem.at[1])
     residual_out[...] = jnp.concatenate([owned_s[j].astype(F32) for j in range(n)], axis=1)
-    drain(sent + back + there + home)
-    finish(last)
-    drain(last)
+    departed(all_s.at[most], send_sem.at[0])
+    departed(proj_s.at[most], send_sem.at[1])
+    for i in range(heads):
+        departed(mix_s.at[0, most], send_sem.at[2 + i])
+    departed(needed_s.at[most], send_sem.at[2 + heads])
+    departed(own_s.at[most], send_sem.at[3 + heads])
+    arrived(out_s.at[most], group_sem.at[2])
+    departed(out_s.at[most], send_sem.at[4 + heads])
 
 
 def combine_kernel(
@@ -318,12 +339,9 @@
     n, slots, width = results.shape
     rows, heads = new_max_in.shape
 
-    def save(h, s):
-        return pltpu.make_async_copy(memory.at[s, h], new_memory.at[s, h], mem_sem.at[h, s])
-
     for h in range(heads):
         for s in range(rows):
-            save(h, s).start()
+            pltpu.make_async_copy(memory.at[s, h], new_memory.at[s, h], mem_sem).start()
     top_s[...] = new_max_in[...]
     top = pltpu.make_async_copy(top_s, max_out, sem.at[0])
     top.start()
@@ -337,9 +355,7 @@
     out_s[...] = (residual[...] + total).astype(BF16)
     out = pltpu.make_async_copy(out_s, layer_out, sem.at[1])
     out.start()
-    for h in range(heads):
-        for s in range(rows):
-            save(h, s).wait()
+    pltpu.make_async_copy(memory, new_memory, mem_sem).wait()
     top.wait()
     out.wait()
 
@@ -398,21 +414,25 @@
             pltpu.VMEM((n * rows, columns), F32),
             pltpu.VMEM((n, rows, total_cols), BF16),
             pltpu.VMEM((n, rows, total_cols), BF16),
-            pltpu.VMEM((heads * key_size, padded), F32),
-            pltpu.VMEM((heads * key_size, padded), F32),
+            pltpu.VMEM((heads, rows, key_size), F32),
+            pltpu.VMEM((heads, key_size, padded), F32),
             pltpu.VMEM((heads, rows, value_size), F32),
             pltpu.VMEM((heads, rows, value_size), F32),
             pltpu.VMEM((heads, rows, value_size), F32),
-            pltpu.VMEM((n, rows, width), BF16),
+            pltpu.VMEM((heads, n, rows, value_size), BF16),
             pltpu.VMEM((n * wanted, columns), BF16),
             pltpu.VMEM((n, wanted, columns), BF16),
             pltpu.VMEM((n, rows, columns), BF16),
             pltpu.VMEM((n, rows, columns), BF16),
             pltpu.VMEM((n, SLOTS, width), BF16),
             pltpu.SemaphoreType.DMA((18,)),
-            pltpu.SemaphoreType.DMA((heads, rows)),
-            pltpu.SemaphoreType.DMA((6, n)),
-            pltpu.SemaphoreType.DMA((6, n)),
+            pltpu.SemaphoreType.DMA,
+            pltpu.SemaphoreType.DMA((5 + heads,)),
+            pltpu.SemaphoreType.DMA((heads, n // 2)),
+            pltpu.SemaphoreType.DMA((heads,)),
+            pltpu.SemaphoreType.DMA((heads,)),
+            pltpu.SemaphoreType.DMA((heads,)),
+            pltpu.SemaphoreType.DMA((3,)),
         ],
         compiler_params=pltpu.CompilerParams(
             collective_id=0, has_side_effects=True, vmem_limit_bytes=40 << 20
@@ -435,7 +455,7 @@
         scratch_shapes=[
             pltpu.VMEM((rows, width), BF16),
             pltpu.VMEM((rows, heads), F32),
-            pltpu.SemaphoreType.DMA((heads, rows)),
+            pltpu.SemaphoreType.DMA,
             pltpu.SemaphoreType.DMA((2,)),
         ],
         compiler_params=pltpu.CompilerParams(vmem_limit_bytes=8 << 20),

time: 41.6 us -> 38.3 us (0.921)
  Pallas kernels: 40.7 us -> 37.4 us
    pallas_call x1, Pallas kernels: 37.3 us -> 34.1 us  [body(): pl.pallas_call(functools.partial(layer_kernel, n, heads, key_size, value_...]
where the time goes in v2:
time: 38.3 us; the launch traced here: 38 us
  Pallas kernels  37.4 us (98%)
  between operations  0.65 us (2%)
    pallas_call x1, Pallas kernels, body(): pl.pallas_call(functools.partial(layer_kernel, n, heads, key_size, value_...  34.1 us
    pallas_call x1, Pallas kernels, body(): pl.pallas_call(combine_kernel, out_shape=(sds((rows, width), BF16), sds(m...  3.32 us

profile of v2, /device:TPU:0, one launch (start us, length us, event | category | flops | bytes accessed | tf_op | source)
XLA Modules:
  0.0 38.0 jit_solution(5232303622120319156)
XLA Ops:
  0.6 34.1 %layer.1 = (f32[4,4,256,512]{3,2,1,0:T(8,128)S(1)}, bf16[16,2,2048]{2,1,0:T(2,128)(2,1)S(1)}, f32[4,2048]{1,0:T(4,128)S(1)}, f32[4,128]{1,0:T(4,128)S(1)}, f32[4,4]{1,0:T(4,128)S(1)}) custom-call(bf16[4,2048]{1,0:T(4,128)(2,1)} %tokens.1, f32[4,4,256,512]{3,2,1,0:T(8,128)} %memory.1, f32[4,4]{1,0:T(4,128)} %max_state.1, f32[1,2048]{1,0:T(1,128)} %bitcast.12, ...), custom_call_target="tpu_custom_call" | custom-call | tf_op jit(solution)/shard_map/layer/pallas_call | solution.py:381
  34.7 3.3 %combine.1 = (bf16[4,2048]{1,0:T(4,128)(2,1)}, f32[4,4,256,512]{3,2,1,0:T(8,128)}, f32[4,4]{1,0:T(4,128)}) custom-call(f32[4,4,256,512]{3,2,1,0:T(8,128)S(1)} %get-tuple-element.8.memory, bf16[16,2,2048]{2,1,0:T(2,128)(2,1)S(1)} %get-tuple-element.9.results, f32[4,2048]{1,0:T(4,128)S(1)} %get-tuple-element.10.residual, ...), custom_call_target="tpu_custom_call" | custom-call | tf_op jit(solution)/shard_map/combine/pallas_call | solution.py:450

commit v3 on v2

--- a/solution.py
+++ b/solution.py
@@ -41,9 +41,13 @@
         remote(source(peer), landing.at[me], send_sem, recv_sem(mask), peer).start()
 
 
+def landed(blocks, sem):
+    pltpu.make_async_copy(blocks, blocks, sem).wait()
+
+
 def spread(n, me, source, target, send_sem, far_sem, near_sem):
     for mask in [*range(n - 2, 0, -2), 1]:
-        sem = near_sem if mask == 1 else far_sem.at[mask // 2]
+        sem = near_sem if mask == 1 else far_sem.at[mask // 2 - 1]
         remote(source, target, send_sem, sem, flip(me, mask)).start()
 
 
@@ -51,9 +55,9 @@
     partner = flip(me, 1)
     for mask in range(2, n, 2):
         block = block_of(mask)
-        piece = remote(block, block, send_sem, far_sem.at[mask // 2], partner)
+        piece = remote(block, block, send_sem, far_sem.at[mask // 2 - 1], partner)
         piece.wait_recv()
-        remote(block, block, send_sem, near_sem, partner).start()
+        remote(block, block, send_sem, near_sem(mask), partner).start()
 
 
 def arrived(blocks, sem):
@@ -101,11 +105,11 @@
     tokens, memory, max_state, norm_gain, wv, wg, wq, wk, w_in, w_forget, forget_bias,
     head_gain, wo, expert_norm, routed, route_weights, w_gate, w_lift, w_down,
     new_memory, results, residual_out, picks_out, max_out,
-    tok_s, max_s, ngain_s, v_w, g_w, q_w, k_w, in_w, forget_w, bias_s,
-    hgain_s, o_w, egain_s, routed_s, rw_s, gate_w, lift_w, down_w,
-    all_s, names_s, pick_s, x_s, proj_s, back_s, k_s, kt_s, v_s, c_s, w_s, mix_s,
+    tok_s, max_s, ngain_s, vg_w, qk_w, gates_w, bias_s,
+    hgain_s, o_w, egain_s, routed_s, rw_s, up_w, down_w,
+    all_s, names_s, pick_s, x_s, proj_s, back_s, kt_s, v_s, c_s, w_s, mix_s,
     res_s, needed_s, own_s, owned_s, out_s,
-    local_sem, mem_sem, send_sem, far_sem, near_sem, column_sem, part_sem, group_sem,
+    local_sem, send_sem, far_sem, near_sem, column_sem, part_sem, group_sem,
 ):
     me = lax.axis_index("ep")
     barrier = pltpu.get_barrier_semaphore()
@@ -113,25 +117,26 @@
         pl.semaphore_signal(barrier, inc=1, device_id={"ep": flip(me, mask)})
     rows, width = tokens.shape
     most = pl.ds(0, n - 1)
-    pairs = [
-        (tokens, tok_s.at[:, pl.ds(0, width)]), (routed, routed_s), (norm_gain, ngain_s),
-        (w_in, in_w), (w_forget, forget_w), (forget_bias, bias_s), (max_state, max_s),
-        (route_weights, rw_s), (wv, v_w), (wg, g_w), (wq, q_w), (wk, k_w),
-        (head_gain, hgain_s), (expert_norm, egain_s), (wo, o_w),
-        (w_gate.at[0], gate_w), (w_lift.at[0], lift_w), (w_down.at[0], down_w),
+    cq, cv = heads * key_size // n, heads * value_size // n
+    flat = cv % 128 == 0
+    halves = [vg_w.at[:, pl.ds(i * cv, cv)] if flat else vg_w.at[pl.ds(i * cv, cv)] for i in range(2)]
+    loads = [
+        (tokens, tok_s, 0), (routed, routed_s, 1), (norm_gain, ngain_s, 2),
+        (w_in, gates_w.at[0], 3), (w_forget, gates_w.at[1], 3), (forget_bias, bias_s, 4),
+        (max_state, max_s, 5), (route_weights, rw_s, 6), (wv, halves[0], 7), (wg, halves[1], 7),
+        (wq, qk_w.at[pl.ds(0, cq)], 8), (wk, qk_w.at[pl.ds(cq, cq)], 8),
+        *(
+            (memory.at[s, h], new_memory.at[s, h], 9)
+            for h in range(heads) for s in range(rows)
+        ),
+        (head_gain, hgain_s, 10), (wo, o_w, 10 + 1), (expert_norm, egain_s, 12),
+        (w_gate.at[0], up_w.at[0], 13), (w_lift.at[0], up_w.at[1], 13), (w_down.at[0], down_w, 14),
     ]
-    loads = [pltpu.make_async_copy(a, b, local_sem.at[i]) for i, (a, b) in enumerate(pairs)]
-    for load in loads[:12]:
-        load.start()
-
-    for h in range(heads):
-        for s in range(rows):
-            pltpu.make_async_copy(memory.at[s, h], new_memory.at[s, h], mem_sem).start()
-    for load in loads[12:]:
-        load.start()
-
-    for load in loads[:8]:
-        load.wait()
+    for source, target, i in loads:
+        pltpu.make_async_copy(source, target, local_sem.at[i]).start()
+
+    for i, target in enumerate((tok_s, routed_s, ngain_s, gates_w, bias_s, max_s, rw_s)):
+        landed(target, local_sem.at[i])
     lane = lax.broadcasted_iota(jnp.int32, (rows, names_width), 1)
     which = routed_s[...]
     weights = rw_s[...]
@@ -149,13 +154,14 @@
         chosen.append(named[r : r + 1] * (taken == slot_of).astype(F32))
         taken = taken + named[r : r + 1]
     chosen = jnp.concatenate(chosen, axis=0)
-    tok_s[:, width:] = chosen.astype(BF16)
+    for j in range(n):
+        proj_s[j, :, :names_width] = chosen.astype(BF16)
     picks_out[...] = chosen * weighed
 
     gain = ngain_s[...]
-    own = scaled_norm(tok_s[:, :width].astype(F32), gain).astype(BF16)
-    input_logit = across(own, in_w[...])
-    raw = across(own, forget_w[...]) + bias_s[...]
+    own = scaled_norm(tok_s[...].astype(F32), gain).astype(BF16)
+    input_logit = across(own, gates_w[0])
+    raw = across(own, gates_w[1]) + bias_s[...]
     log_forget = jnp.minimum(raw, 0.0) - jnp.log1p(jnp.exp(-jnp.abs(raw)))
     prior = log_forget + max_s[...]
     new_max = jnp.maximum(prior, input_logit)
@@ -166,30 +172,87 @@
     pl.semaphore_wait(barrier, n - 1)
     spread(n, me, tok_s, all_s.at[me], send_sem.at[0], far_sem.at[0], near_sem.at[0])
     all_s[me] = tok_s[...]
-    for load in loads[8:12]:
-        load.wait()
+    landed(vg_w, local_sem.at[7])
+    landed(qk_w, local_sem.at[8])
     relay(
-        n, me, lambda mask: all_s.at[flip(me, mask)], send_sem.at[0], far_sem.at[0], near_sem.at[0]
-    )
-    arrived(all_s.at[pl.ds(0, n // 2)], near_sem.at[0])
-    normed = scaled_norm(rows_of(all_s, n, 0, width), gain).astype(BF16)
-    cq, cv = heads * key_size // n, heads * value_size // n
-    tables = [v_w[...], g_w[...], q_w[...], k_w[...]]
-    projected = jnp.concatenate(
-        [apply(normed, table, c) for table, c in zip(tables, (cv, cv, cq, cq))], axis=1
-    )
-    for j in range(n):
-        proj_s[j] = projected[j * rows : (j + 1) * rows].astype(BF16)
+        n, me, lambda mask: all_s.at[flip(me, mask)], send_sem.at[0], far_sem.at[0],
+        lambda mask: near_sem.at[0 if mask < n // 2 else heads],
+    )
     per = n // heads
-    exchange(
-        n, me, lambda peer: proj_s.at[peer], back_s, send_sem.at[1],
-        lambda mask: column_sem.at[mask // per],
-    )
+
+    def project(origins):
+        entries = jnp.concatenate([all_s[j].astype(F32) for j in origins], axis=0)
+        entries = scaled_norm(entries, gain).astype(BF16)
+        for table, start in ((vg_w, names_width), (qk_w, names_width + 2 * cv)):
+            made = apply(entries, table[...], table.shape[1] if flat and table is vg_w else 1)
+            for i, j in enumerate(origins):
+                proj_s[j, :, start : start + made.shape[1]] = (
+                    made[i * rows : (i + 1) * rows].astype(BF16)
+                )
+
+    def reply(masks):
+        for mask in masks:
+            peer = flip(me, mask)
+            remote(
+                proj_s.at[peer], back_s.at[me], send_sem.at[1], column_sem.at[mask // per], peer
+            ).start()
+
+    early = [*range(n // 2), *range(n // 2, n, 2)]
+    late = [*range(n // 2 + 1, n, 2)]
+    arrived(all_s.at[pl.ds(0, n // 4)], near_sem.at[0])
+    project([flip(me, mask) for mask in early])
+    reply(early[:0:-1])
+    arrived(all_s.at[pl.ds(0, n // 4)], near_sem.at[heads])
+    project([flip(me, mask) for mask in late])
+    reply(late[::-1])
     back_s[me] = proj_s[me]
 
     columns = res_s.shape[1]
     x_s[...] = own_columns(all_s, n, me, columns)
-    names_s[...] = rows_of(all_s, n, width, names_width).T
+    for i, target in ((10, hgain_s), (11, o_w), (12, egain_s)):
+        landed(target, local_sem.at[i])
+    pltpu.make_async_copy(memory, new_memory, local_sem.at[9]).wait()
+    for h in range(heads):
+        c_s[h] = jnp.broadcast_to(carried[:, h : h + 1], (rows, value_size))
+        w_s[h] = jnp.broadcast_to(written[:, h : h + 1], (rows, value_size))
+    step = 32
+    quarter = lax.div(me, per)
+    pad = jnp.zeros((-rows % 8, 2 * key_size), F32)
+
+    def read(h):
+        pieces = [back_s[h * per + t][:, names_width:].astype(F32) for t in range(per)]
+        v = jnp.concatenate([b[:, :cv] for b in pieces], axis=1)
+        g = jnp.concatenate([b[:, cv : 2 * cv] for b in pieces], axis=1)
+        qk = jnp.concatenate([b[:, 2 * cv :] for b in pieces], axis=1)
+        turned = jnp.concatenate([qk, pad], axis=0).T
+        query = jnp.concatenate([turned[t * 2 * cq : t * 2 * cq + cq] for t in range(per)], axis=0)
+        key = jnp.concatenate([turned[t * 2 * cq + cq : (t + 1) * 2 * cq] for t in range(per)], axis=0)
+        v = v * w_s[h]
+        match = jnp.sum(query * key, axis=0, keepdims=True)
+        gains = hgain_s[:, pl.ds(pl.multiple_of(h * value_size, value_size), value_size)]
+        gains = gains * jax.nn.sigmoid(g)
+        sums, own_match = [], []
+        for s in range(rows):
+            total = jnp.zeros((8, value_size), F32)
+            for at in range(0, key_size, step):
+                terms = query[at : at + step, s : s + 1] * new_memory[s, h, at : at + step, :]
+                total = total + jnp.sum(terms.reshape(step // 8, 8, value_size), axis=0)
+            sums.append(jnp.sum(total, axis=0, keepdims=True))
+            own_match.append(match[:, s : s + 1] * v[s : s + 1])
+        readout = c_s[h] * jnp.concatenate(sums, axis=0) + jnp.concatenate(own_match, axis=0)
+        return scaled_norm(readout, gains).astype(BF16), key, v
+
+    for i in range(heads):
+        arrived(back_s.at[pl.ds(0, per if i else per - 1)], column_sem.at[i])
+        h = flip(quarter, i)
+        mix_s[h, me], kt_s[h], v_s[h] = read(h)
+        mine = mix_s.at[h, me]
+        if i < heads - 1:
+            spread(n, me, mine, mine, send_sem.at[2 + i], far_sem.at[1 + i], near_sem.at[1 + i])
+        else:
+            for mask in range(n - 1, 0, -1):
+                remote(mine, mine, send_sem.at[2 + i], group_sem.at[0], flip(me, mask)).start()
+    names_s[...] = rows_of(back_s, n, 0, names_width).T
     wanted = SLOTS * n
     place = lax.broadcasted_iota(jnp.int32, (wanted, n * rows), 0)
     row = lax.broadcasted_iota(jnp.int32, (wanted, n * rows), 1)
@@ -199,47 +262,6 @@
     for j in range(n):
         value = jnp.where(even, names_s[j : j + 1, :], names_s[n + j : n + j + 1, :])
         pick_s[j] = jnp.where(inside, value, 0.0).astype(BF16)
-    for load in loads[12:15]:
-        load.wait()
-    pltpu.make_async_copy(memory, new_memory, mem_sem).wait()
-    for h in range(heads):
-        c_s[h] = jnp.broadcast_to(carried[:, h : h + 1], (rows, value_size))
-        w_s[h] = jnp.broadcast_to(written[:, h : h + 1], (rows, value_size))
-    step = 32
-    quarter = lax.div(me, per)
-    pad = jnp.zeros((-rows % 8, key_size), F32)
-
-    def read(h):
-        pieces = [back_s[h * per + t].astype(F32) for t in range(per)]
-        v = jnp.concatenate([b[:, :cv] for b in pieces], axis=1)
-        g = jnp.concatenate([b[:, cv : 2 * cv] for b in pieces], axis=1)
-        q = jnp.concatenate([b[:, 2 * cv : 2 * cv + cq] for b in pieces], axis=1)
-        k = jnp.concatenate([b[:, 2 * cv + cq :] for b in pieces], axis=1)
-        query = jnp.concatenate([q, pad], axis=0).T
-        v = v * w_s[h]
-        match = jnp.sum(q * k, axis=1, keepdims=True) * v
-        gains = hgain_s[:, pl.ds(pl.multiple_of(h * value_size, value_size), value_size)]
-        gains = gains * jax.nn.sigmoid(g)
-        sums = []
-        for s in range(rows):
-            total = jnp.zeros((8, value_size), F32)
-            for at in range(0, key_size, step):
-                terms = query[at : at + step, s : s + 1] * new_memory[s, h, at : at + step, :]
-                total = total + jnp.sum(terms.reshape(step // 8, 8, value_size), axis=0)
-            sums.append(jnp.sum(total, axis=0, keepdims=True))
-        readout = c_s[h] * jnp.concatenate(sums, axis=0) + match
-        return scaled_norm(readout, gains).astype(BF16), k, v
-
-    for i in range(heads):
-        arrived(back_s.at[pl.ds(0, per if i else per - 1)], column_sem.at[i])
-        h = flip(quarter, i)
-        mix_s[h, me], k_s[h], v_s[h] = read(h)
-        mine = mix_s.at[h, me]
-        if i < heads - 1:
-            spread(n, me, mine, mine, send_sem.at[2 + i], far_sem.at[1 + i], near_sem.at[1 + i])
-        else:
-            for mask in range(n - 1, 0, -1):
-                remote(mine, mine, send_sem.at[2 + i], group_sem.at[0], flip(me, mask)).start()
 
     def update(h, carry):
         for s in range(rows):
@@ -256,13 +278,11 @@
             lax.fori_loop(0, key_size // step, chunk, 0, unroll=True)
         return carry
 
-    for h in range(heads):
-        kt_s[h] = jnp.concatenate([k_s[h], pad], axis=0).T
     lax.fori_loop(0, heads, update, 0)
     for i in range(heads - 1):
         relay(
             n, me, lambda mask: mix_s.at[flip(quarter, mask // per ^ i), flip(me, mask)],
-            send_sem.at[2 + i], far_sem.at[1 + i], near_sem.at[1 + i],
+            send_sem.at[2 + i], far_sem.at[1 + i], lambda mask: near_sem.at[1 + i],
         )
     for i in range(heads - 1):
         arrived(mix_s.at[0, pl.ds(0, n // 2)], near_sem.at[1 + i])
@@ -288,26 +308,27 @@
     whole = residual.astype(F32)
     for j in range(n):
         own_s[j] = whole[j * rows : (j + 1) * rows].astype(BF16)
-    exchange(
-        n, me, lambda peer: own_s.at[peer], owned_s, send_sem.at[3 + heads],
-        lambda mask: group_sem.at[1],
-    )
     owned_s[me] = own_s[me]
-    for load in loads[15:]:
-        load.wait()
+    landed(up_w, local_sem.at[13])
+    landed(down_w, local_sem.at[14])
     span = per * columns
-    gate_value = jnp.zeros((wanted, gate_w.shape[1]), F32)
-    lift_value = jnp.zeros((wanted, lift_w.shape[1]), F32)
+    gate_value = jnp.zeros((wanted, up_w.shape[2]), F32)
+    lift_value = jnp.zeros((wanted, up_w.shape[2]), F32)
     square = jnp.zeros((wanted, 1), F32)
     for i in range(heads):
         arrived(needed_s.at[pl.ds(0, per if i else per - 1)], part_sem.at[i])
+        if i == heads - 2:
+            exchange(
+                n, me, lambda peer: own_s.at[peer], owned_s, send_sem.at[3 + heads],
+                lambda mask: group_sem.at[1],
+            )
         part = flip(quarter, i)
         block = jnp.concatenate([needed_s[part * per + t].astype(F32) for t in range(per)], axis=1)
         at = pl.ds(pl.multiple_of(part * span, span), span)
         square += jnp.sum(block * block, axis=1, keepdims=True)
         block = (block * egain_s[:, at]).astype(BF16)
-        gate_value += jnp.dot(block, gate_w[at, :], preferred_element_type=F32)
-        lift_value += jnp.dot(block, lift_w[at, :], preferred_element_type=F32)
+        gate_value += jnp.dot(block, up_w[0, at, :], preferred_element_type=F32)
+        lift_value += jnp.dot(block, up_w[1, at, :], preferred_element_type=F32)
     scale = lax.rsqrt(square / width + epsilon)
     gate_value, lift_value = gate_value * scale, lift_value * scale
     hidden = (jax.nn.silu(gate_value) * lift_value).astype(BF16)
@@ -341,7 +362,9 @@
 
     for h in range(heads):
         for s in range(rows):
-            pltpu.make_async_copy(memory.at[s, h], new_memory.at[s, h], mem_sem).start()
+            for at in range(0, memory.shape[2], memory.shape[2] // 4):
+                block = (s, h, pl.ds(at, memory.shape[2] // 4))
+                pltpu.make_async_copy(memory.at[block], new_memory.at[block], mem_sem).start()
     top_s[...] = new_max_in[...]
     top = pltpu.make_async_copy(top_s, max_out, sem.at[0])
     top.start()
@@ -370,10 +393,11 @@
     _, heads, key_size, value_size = memory_state.shape
     hidden = expert_gate.shape[2]
     cq, cv, columns = query_weight.shape[1], value_weight.shape[1], output_weight.shape[1]
-    total_cols = 2 * cq + 2 * cv
-    wv, wg, wq, wk = (tall(t) for t in (value_weight, output_gate, query_weight, key_weight))
-    wo = tall(output_weight)
+    wv, wg, wo = tall(value_weight), tall(output_gate), tall(output_weight)
+    wq, wk = query_weight.T, key_weight.T
+    vg_shape = (width, 2 * cv) if wv.shape[0] == width and cv % 128 == 0 else (2 * cv, width)
     names_width = -(-SLOTS * n // 128) * 128
+    total_cols = names_width + 2 * cq + 2 * cv
     wanted = SLOTS * n
     sds = jax.ShapeDtypeStruct
     small = sds((rows, heads), F32)
@@ -390,31 +414,26 @@
         in_specs=[HBM] * 19,
         out_specs=[VMEM] * 5,
         scratch_shapes=[
-            pltpu.VMEM((rows, width + names_width), BF16),
+            pltpu.VMEM((rows, width), BF16),
             pltpu.VMEM((rows, heads), F32),
             pltpu.VMEM((1, width), F32),
-            pltpu.VMEM(wv.shape, BF16),
-            pltpu.VMEM(wg.shape, BF16),
-            pltpu.VMEM(wq.shape, BF16),
-            pltpu.VMEM(wk.shape, BF16),
-            pltpu.VMEM((heads, width), BF16),
-            pltpu.VMEM((heads, width), BF16),
+            pltpu.VMEM(vg_shape, BF16),
+            pltpu.VMEM((2 * cq, width), BF16),
+            pltpu.VMEM((2, heads, width), BF16),
             pltpu.VMEM((1, heads), F32),
             pltpu.VMEM((1, width), F32),
             pltpu.VMEM(wo.shape, BF16),
             pltpu.VMEM((1, width), F32),
             pltpu.VMEM(routed_experts.shape, jnp.int32),
             pltpu.VMEM(route_weights.shape, F32),
-            pltpu.VMEM((width, hidden), BF16),
-            pltpu.VMEM((width, hidden), BF16),
+            pltpu.VMEM((2, width, hidden), BF16),
             pltpu.VMEM((hidden, width), BF16),
-            pltpu.VMEM((n, rows, width + names_width), BF16),
+            pltpu.VMEM((n, rows, width), BF16),
             pltpu.VMEM((names_width, n * rows), F32),
             pltpu.VMEM((n, wanted, n * rows), BF16),
             pltpu.VMEM((n * rows, columns), F32),
             pltpu.VMEM((n, rows, total_cols), BF16),
             pltpu.VMEM((n, rows, total_cols), BF16),
-            pltpu.VMEM((heads, rows, key_size), F32),
             pltpu.VMEM((heads, key_size, padded), F32),
             pltpu.VMEM((heads, rows, value_size), F32),
             pltpu.VMEM((heads, rows, value_size), F32),
@@ -425,11 +444,10 @@
             pltpu.VMEM((n, rows, columns), BF16),
             pltpu.VMEM((n, rows, columns), BF16),
             pltpu.VMEM((n, SLOTS, width), BF16),
-            pltpu.SemaphoreType.DMA((18,)),
-            pltpu.SemaphoreType.DMA,
+            pltpu.SemaphoreType.DMA((15,)),
             pltpu.SemaphoreType.DMA((5 + heads,)),
-            pltpu.SemaphoreType.DMA((heads, n // 2)),
-            pltpu.SemaphoreType.DMA((heads,)),
+            pltpu.SemaphoreType.DMA((heads, n // 2 - 1)),
+            pltpu.SemaphoreType.DMA((heads + 1,)),
             pltpu.SemaphoreType.DMA((heads,)),
             pltpu.SemaphoreType.DMA((heads,)),
             pltpu.SemaphoreType.DMA((3,)),

time: 38.3 us -> 37.5 us (0.979)
  Pallas kernels: 37.4 us -> 36.6 us
    pallas_call x1, Pallas kernels: 34.1 us -> 33.4 us  [body(): pl.pallas_call(functools.partial(layer_kernel, n, heads, key_size, value_...]
where the time goes in v3:
time: 37.5 us; the launch traced here: 37.3 us
  Pallas kernels  36.6 us (98%)
  between operations  0.65 us (2%)
    pallas_call x1, Pallas kernels, body(): pl.pallas_call(functools.partial(layer_kernel, n, heads, key_size, value_...  33.4 us
    pallas_call x1, Pallas kernels, body(): pl.pallas_call(combine_kernel, out_shape=(sds((rows, width), BF16), sds(m...  3.26 us

profile of v3, /device:TPU:0, one launch (start us, length us, event | category | flops | bytes accessed | tf_op | source)
XLA Modules:
  0.0 37.3 jit_solution(17273264538925230179)
XLA Ops:
  0.6 33.4 %layer.1 = (f32[4,4,256,512]{3,2,1,0:T(8,128)S(1)}, bf16[16,2,2048]{2,1,0:T(2,128)(2,1)S(1)}, f32[4,2048]{1,0:T(4,128)S(1)}, f32[4,128]{1,0:T(4,128)S(1)}, f32[4,4]{1,0:T(4,128)S(1)}) custom-call(bf16[4,2048]{1,0:T(4,128)(2,1)} %tokens.1, f32[4,4,256,512]{3,2,1,0:T(8,128)} %memory.1, f32[4,4]{1,0:T(4,128)} %max_state.1, f32[1,2048]{1,0:T(1,128)} %bitcast.12, ...), custom_call_target="tpu_custom_call" | custom-call | tf_op jit(solution)/shard_map/layer/pallas_call | solution.py:405
  34.0 3.3 %combine.1 = (bf16[4,2048]{1,0:T(4,128)(2,1)}, f32[4,4,256,512]{3,2,1,0:T(8,128)}, f32[4,4]{1,0:T(4,128)}) custom-call(f32[4,4,256,512]{3,2,1,0:T(8,128)S(1)} %get-tuple-element.8.memory, bf16[16,2,2048]{2,1,0:T(2,128)(2,1)S(1)} %get-tuple-element.9.results, f32[4,2048]{1,0:T(4,128)S(1)} %get-tuple-element.10.residual, ...), custom_call_target="tpu_custom_call" | custom-call | tf_op jit(solution)/shard_map/combine/pallas_call | solution.py:468

commit v4 on v3

--- a/solution.py
+++ b/solution.py
@@ -45,19 +45,9 @@
     pltpu.make_async_copy(blocks, blocks, sem).wait()
 
 
-def spread(n, me, source, target, send_sem, far_sem, near_sem):
-    for mask in [*range(n - 2, 0, -2), 1]:
-        sem = near_sem if mask == 1 else far_sem.at[mask // 2 - 1]
-        remote(source, target, send_sem, sem, flip(me, mask)).start()
-
-
-def relay(n, me, block_of, send_sem, far_sem, near_sem):
-    partner = flip(me, 1)
-    for mask in range(2, n, 2):
-        block = block_of(mask)
-        piece = remote(block, block, send_sem, far_sem.at[mask // 2 - 1], partner)
-        piece.wait_recv()
-        remote(block, block, send_sem, near_sem(mask), partner).start()
+def spread(n, me, source, target, send_sem, recv_sem):
+    for mask in range(n - 2, 0, -2):
+        remote(source(mask), target, send_sem, recv_sem(mask), flip(me, mask)).start()
 
 
 def arrived(blocks, sem):
@@ -76,28 +66,14 @@
     return lax.dot_general(lhs, table, (((1,), (1,)), ((), ())), preferred_element_type=F32)
 
 
-def apply(lhs, table, columns):
-    if columns % 128 == 0:
+def apply(lhs, table):
+    if table.shape[0] == lhs.shape[1]:
         return jnp.dot(lhs, table, preferred_element_type=F32)
     return across(lhs, table)
 
 
 def rows_of(ref, n, start, size):
     return jnp.concatenate([ref[j, :, start : start + size].astype(F32) for j in range(n)], axis=0)
-
-
-def own_columns(ref, n, me, columns):
-    if columns % 128 == 0:
-        at = pl.ds(pl.multiple_of(me * columns, 128), columns)
-        return jnp.concatenate([ref[j, :, at].astype(F32) for j in range(n)], axis=0)
-    share = 128 // columns
-    at = pl.ds(pl.multiple_of(lax.div(me, share) * 128, 128), 128)
-    wide = jnp.concatenate([ref[j, :, at].astype(F32) for j in range(n)], axis=0)
-    part = lax.rem(me, share)
-    picked = wide[:, :columns]
-    for i in range(1, share):
-        picked = jnp.where(part == i, wide[:, i * columns : (i + 1) * columns], picked)
-    return picked
 
 
 def layer_kernel(
@@ -109,27 +85,38 @@
     hgain_s, o_w, egain_s, routed_s, rw_s, up_w, down_w,
     all_s, names_s, pick_s, x_s, proj_s, back_s, kt_s, v_s, c_s, w_s, mix_s,
     res_s, needed_s, own_s, owned_s, out_s,
-    local_sem, send_sem, far_sem, near_sem, column_sem, part_sem, group_sem,
+    local_sem, send_sem, column_sem, part_sem, group_sem,
 ):
     me = lax.axis_index("ep")
     barrier = pltpu.get_barrier_semaphore()
     for mask in range(n - 1, 0, -1):
         pl.semaphore_signal(barrier, inc=1, device_id={"ep": flip(me, mask)})
     rows, width = tokens.shape
-    most = pl.ds(0, n - 1)
+    most, same = pl.ds(0, n - 1), pl.ds(0, n // 2 - 1)
+    core, chip = lax.rem(me, 2), lax.div(me, 2)
     cq, cv = heads * key_size // n, heads * value_size // n
-    flat = cv % 128 == 0
-    halves = [vg_w.at[:, pl.ds(i * cv, cv)] if flat else vg_w.at[pl.ds(i * cv, cv)] for i in range(2)]
+    columns = wo.shape[1] if wo.shape[0] == width else wo.shape[0]
+
+    def part_of(table, size, start, count):
+        at = pl.ds(pl.multiple_of(core * size, size) + start, count)
+        return table.at[:, at] if table.shape[0] == width else table.at[at]
+
+    shared = [
+        part_of(vg_w, 2 * cv, 0, 2 * cv), part_of(qk_w, 2 * cq, 0, 2 * cq),
+        part_of(o_w, columns, 0, columns),
+    ]
     loads = [
         (tokens, tok_s, 0), (routed, routed_s, 1), (norm_gain, ngain_s, 2),
         (w_in, gates_w.at[0], 3), (w_forget, gates_w.at[1], 3), (forget_bias, bias_s, 4),
-        (max_state, max_s, 5), (route_weights, rw_s, 6), (wv, halves[0], 7), (wg, halves[1], 7),
-        (wq, qk_w.at[pl.ds(0, cq)], 8), (wk, qk_w.at[pl.ds(cq, cq)], 8),
+        (max_state, max_s, 5), (route_weights, rw_s, 6), (wv, part_of(vg_w, 2 * cv, 0, cv), 7),
+        (wg, part_of(vg_w, 2 * cv, cv, cv), 7),
+        (wq, part_of(qk_w, 2 * cq, 0, cq), 8),
+        (wk, part_of(qk_w, 2 * cq, cq, cq), 8), (wo, shared[2], 10 + 1),
         *(
             (memory.at[s, h], new_memory.at[s, h], 9)
             for h in range(heads) for s in range(rows)
         ),
-        (head_gain, hgain_s, 10), (wo, o_w, 10 + 1), (expert_norm, egain_s, 12),
+        (head_gain, hgain_s, 10), (expert_norm, egain_s, 12),
         (w_gate.at[0], up_w.at[0], 13), (w_lift.at[0], up_w.at[1], 13), (w_down.at[0], down_w, 14),
     ]
     for source, target, i in loads:
@@ -154,8 +141,9 @@
         chosen.append(named[r : r + 1] * (taken == slot_of).astype(F32))
         taken = taken + named[r : r + 1]
     chosen = jnp.concatenate(chosen, axis=0)
-    for j in range(n):
-        proj_s[j, :, :names_width] = chosen.astype(BF16)
+    for t in range(n // 2):
+        for c in range(2):
+            proj_s[t, c, :, :names_width] = chosen.astype(BF16)
     picks_out[...] = chosen * weighed
 
     gain = ngain_s[...]
@@ -170,46 +158,34 @@
     written = jnp.exp(input_logit - new_max) * key_size**-0.5
 
     pl.semaphore_wait(barrier, n - 1)
-    spread(n, me, tok_s, all_s.at[me], send_sem.at[0], far_sem.at[0], near_sem.at[0])
-    all_s[me] = tok_s[...]
-    landed(vg_w, local_sem.at[7])
-    landed(qk_w, local_sem.at[8])
-    relay(
-        n, me, lambda mask: all_s.at[flip(me, mask)], send_sem.at[0], far_sem.at[0],
-        lambda mask: near_sem.at[0 if mask < n // 2 else heads],
-    )
+    spread(n, me, lambda mask: tok_s, all_s.at[chip], send_sem.at[0], lambda mask: group_sem.at[0])
+    all_s[chip] = tok_s[...]
+    partner = flip(me, 1)
+    for i, block in enumerate(shared):
+        landed(block, local_sem.at[(7, 8, 11)[i]])
+        remote(block, block, send_sem.at[5 + heads + i], group_sem.at[3 + i], partner).start()
     per = n // heads
-
-    def project(origins):
-        entries = jnp.concatenate([all_s[j].astype(F32) for j in origins], axis=0)
-        entries = scaled_norm(entries, gain).astype(BF16)
-        for table, start in ((vg_w, names_width), (qk_w, names_width + 2 * cv)):
-            made = apply(entries, table[...], table.shape[1] if flat and table is vg_w else 1)
-            for i, j in enumerate(origins):
-                proj_s[j, :, start : start + made.shape[1]] = (
-                    made[i * rows : (i + 1) * rows].astype(BF16)
+    arrived(shared[0], group_sem.at[3])
+    arrived(shared[1], group_sem.at[4])
+    arrived(all_s.at[same], group_sem.at[0])
+    entries = jnp.concatenate([all_s[t].astype(F32) for t in range(n // 2)], axis=0)
+    entries = scaled_norm(entries, gain).astype(BF16)
+    for table, start, size in ((vg_w, names_width, 2 * cv), (qk_w, names_width + 2 * cv, 2 * cq)):
+        made = apply(entries, table[...]).astype(BF16).astype(F32)
+        for t in range(n // 2):
+            for c in range(2):
+                proj_s[t, c, :, start : start + size] = (
+                    made[t * rows : (t + 1) * rows, c * size : (c + 1) * size].astype(BF16)
                 )
-
-    def reply(masks):
-        for mask in masks:
-            peer = flip(me, mask)
-            remote(
-                proj_s.at[peer], back_s.at[me], send_sem.at[1], column_sem.at[mask // per], peer
-            ).start()
-
-    early = [*range(n // 2), *range(n // 2, n, 2)]
-    late = [*range(n // 2 + 1, n, 2)]
-    arrived(all_s.at[pl.ds(0, n // 4)], near_sem.at[0])
-    project([flip(me, mask) for mask in early])
-    reply(early[:0:-1])
-    arrived(all_s.at[pl.ds(0, n // 4)], near_sem.at[heads])
-    project([flip(me, mask) for mask in late])
-    reply(late[::-1])
-    back_s[me] = proj_s[me]
-
-    columns = res_s.shape[1]
-    x_s[...] = own_columns(all_s, n, me, columns)
-    for i, target in ((10, hgain_s), (11, o_w), (12, egain_s)):
+    spread(
+        n, me, lambda mask: proj_s.at[flip(chip, mask // 2)], back_s.at[chip], send_sem.at[1],
+        lambda mask: column_sem.at[mask // per],
+    )
+    back_s[chip] = proj_s[chip]
+
+    at = pl.ds(pl.multiple_of(chip * 2 * columns, 2 * columns), 2 * columns)
+    x_s[...] = jnp.concatenate([all_s[t, :, at].astype(F32) for t in range(n // 2)], axis=0)
+    for i, target in ((10, hgain_s), (12, egain_s)):
         landed(target, local_sem.at[i])
     pltpu.make_async_copy(memory, new_memory, local_sem.at[9]).wait()
     for h in range(heads):
@@ -220,7 +196,9 @@
     pad = jnp.zeros((-rows % 8, 2 * key_size), F32)
 
     def read(h):
-        pieces = [back_s[h * per + t][:, names_width:].astype(F32) for t in range(per)]
+        pieces = [
+            back_s[h * (per // 2) + t // 2, t % 2][:, names_width:].astype(F32) for t in range(per)
+        ]
         v = jnp.concatenate([b[:, :cv] for b in pieces], axis=1)
         g = jnp.concatenate([b[:, cv : 2 * cv] for b in pieces], axis=1)
         qk = jnp.concatenate([b[:, 2 * cv :] for b in pieces], axis=1)
@@ -243,19 +221,19 @@
         return scaled_norm(readout, gains).astype(BF16), key, v
 
     for i in range(heads):
-        arrived(back_s.at[pl.ds(0, per if i else per - 1)], column_sem.at[i])
+        count = per // 2 if i else per // 2 - 1
+        if count:
+            arrived(back_s.at[pl.ds(0, count)], column_sem.at[i])
         h = flip(quarter, i)
-        mix_s[h, me], kt_s[h], v_s[h] = read(h)
-        mine = mix_s.at[h, me]
-        if i < heads - 1:
-            spread(n, me, mine, mine, send_sem.at[2 + i], far_sem.at[1 + i], near_sem.at[1 + i])
-        else:
-            for mask in range(n - 1, 0, -1):
-                remote(mine, mine, send_sem.at[2 + i], group_sem.at[0], flip(me, mask)).start()
-    names_s[...] = rows_of(back_s, n, 0, names_width).T
-    wanted = SLOTS * n
-    place = lax.broadcasted_iota(jnp.int32, (wanted, n * rows), 0)
-    row = lax.broadcasted_iota(jnp.int32, (wanted, n * rows), 1)
+        mix_s[h, chip], kt_s[h], v_s[h] = read(h)
+        mine = mix_s.at[h, chip]
+        spread(n, me, lambda mask: mine, mine, send_sem.at[2], lambda mask: group_sem.at[6])
+    names_s[...] = jnp.concatenate(
+        [back_s[t, 0][:, :names_width].astype(F32) for t in range(n // 2)], axis=0
+    ).T
+    wanted = SLOTS * n // 2
+    place = lax.broadcasted_iota(jnp.int32, (wanted, n // 2 * rows), 0)
+    row = lax.broadcasted_iota(jnp.int32, (wanted, n // 2 * rows), 1)
     first = (place - place % SLOTS) // SLOTS * rows
     inside = (row >= first) & (row < first + rows)
     even = place % SLOTS == 0
@@ -279,25 +257,19 @@
         return carry
 
     lax.fori_loop(0, heads, update, 0)
-    for i in range(heads - 1):
-        relay(
-            n, me, lambda mask: mix_s.at[flip(quarter, mask // per ^ i), flip(me, mask)],
-            send_sem.at[2 + i], far_sem.at[1 + i], lambda mask: near_sem.at[1 + i],
-        )
-    for i in range(heads - 1):
-        arrived(mix_s.at[0, pl.ds(0, n // 2)], near_sem.at[1 + i])
-    arrived(mix_s.at[0, most], group_sem.at[0])
+    arrived(mix_s.at[:, same], group_sem.at[6])
+    arrived(shared[2], group_sem.at[5])
     mixed = jnp.concatenate(
         [
-            jnp.concatenate([mix_s[h, j].astype(F32) for j in range(n)], axis=0).astype(BF16)
+            jnp.concatenate([mix_s[h, t].astype(F32) for t in range(n // 2)], axis=0).astype(BF16)
             for h in range(heads)
         ],
         axis=1,
     )
-    branch = apply(mixed, o_w[...], columns).astype(BF16)
+    branch = apply(mixed, o_w[...]).astype(BF16)
     residual = (x_s[...] + branch.astype(F32)).astype(BF16)
     picked = jnp.dot(
-        pick_s[...].reshape(n * wanted, n * rows), residual, preferred_element_type=F32
+        pick_s[...].reshape(n * wanted, n // 2 * rows), residual, preferred_element_type=F32
     ).astype(BF16)
     res_s[...] = picked
     exchange(
@@ -306,24 +278,32 @@
     )
     needed_s[me] = res_s[pl.ds(pl.multiple_of(me * wanted, wanted), wanted)]
     whole = residual.astype(F32)
-    for j in range(n):
-        own_s[j] = whole[j * rows : (j + 1) * rows].astype(BF16)
-    owned_s[me] = own_s[me]
+    for t in range(n // 2):
+        own_s[t] = whole[t * rows : (t + 1) * rows].astype(BF16)
+    owned_s[chip] = own_s[chip]
     landed(up_w, local_sem.at[13])
     landed(down_w, local_sem.at[14])
     span = per * columns
-    gate_value = jnp.zeros((wanted, up_w.shape[2]), F32)
-    lift_value = jnp.zeros((wanted, up_w.shape[2]), F32)
-    square = jnp.zeros((wanted, 1), F32)
+    gate_value = jnp.zeros((2 * wanted, up_w.shape[2]), F32)
+    lift_value = jnp.zeros((2 * wanted, up_w.shape[2]), F32)
+    square = jnp.zeros((2 * wanted, 1), F32)
     for i in range(heads):
         arrived(needed_s.at[pl.ds(0, per if i else per - 1)], part_sem.at[i])
         if i == heads - 2:
-            exchange(
-                n, me, lambda peer: own_s.at[peer], owned_s, send_sem.at[3 + heads],
-                lambda mask: group_sem.at[1],
+            spread(
+                n, me, lambda mask: own_s.at[flip(chip, mask // 2)], owned_s.at[chip],
+                send_sem.at[3 + heads], lambda mask: group_sem.at[1],
             )
         part = flip(quarter, i)
-        block = jnp.concatenate([needed_s[part * per + t].astype(F32) for t in range(per)], axis=1)
+        block = jnp.concatenate(
+            [
+                jnp.concatenate(
+                    [needed_s[part * per + t + c].astype(F32) for t in range(0, per, 2)], axis=1
+                )
+                for c in range(2)
+            ],
+            axis=0,
+        )
         at = pl.ds(pl.multiple_of(part * span, span), span)
         square += jnp.sum(block * block, axis=1, keepdims=True)
         block = (block * egain_s[:, at]).astype(BF16)
@@ -334,20 +314,22 @@
     hidden = (jax.nn.silu(gate_value) * lift_value).astype(BF16)
     result = jnp.dot(hidden, down_w[...], preferred_element_type=F32)
     for j in range(n):
-        out_s[j] = result[j * SLOTS : (j + 1) * SLOTS].astype(BF16)
+        at = j % 2 * wanted + j // 2 * SLOTS
+        out_s[j] = result[at : at + SLOTS].astype(BF16)
     exchange(
         n, me, lambda peer: out_s.at[peer], results, send_sem.at[4 + heads],
         lambda mask: group_sem.at[2],
     )
     results[me] = out_s[me]
-    arrived(owned_s.at[most], group_sem.at[1])
-    residual_out[...] = jnp.concatenate([owned_s[j].astype(F32) for j in range(n)], axis=1)
-    departed(all_s.at[most], send_sem.at[0])
-    departed(proj_s.at[most], send_sem.at[1])
-    for i in range(heads):
-        departed(mix_s.at[0, most], send_sem.at[2 + i])
+    arrived(owned_s.at[same], group_sem.at[1])
+    residual_out[...] = jnp.concatenate([owned_s[t].astype(F32) for t in range(n // 2)], axis=1)
+    departed(all_s.at[same], send_sem.at[0])
+    departed(proj_s.at[same], send_sem.at[1])
+    departed(mix_s.at[:, same], send_sem.at[2])
+    for i, block in enumerate(shared):
+        departed(block, send_sem.at[5 + heads + i])
     departed(needed_s.at[most], send_sem.at[2 + heads])
-    departed(own_s.at[most], send_sem.at[3 + heads])
+    departed(own_s.at[same], send_sem.at[3 + heads])
     arrived(out_s.at[most], group_sem.at[2])
     departed(out_s.at[most], send_sem.at[4 + heads])
 
@@ -395,10 +377,11 @@
     cq, cv, columns = query_weight.shape[1], value_weight.shape[1], output_weight.shape[1]
     wv, wg, wo = tall(value_weight), tall(output_gate), tall(output_weight)
     wq, wk = query_weight.T, key_weight.T
-    vg_shape = (width, 2 * cv) if wv.shape[0] == width and cv % 128 == 0 else (2 * cv, width)
+    vg_shape = (width, 4 * cv) if cv % 128 == 0 else (4 * cv, width)
+    o_shape = (width, 2 * columns) if columns % 128 == 0 else (2 * columns, width)
     names_width = -(-SLOTS * n // 128) * 128
     total_cols = names_width + 2 * cq + 2 * cv
-    wanted = SLOTS * n
+    wanted = SLOTS * n // 2
     sds = jax.ShapeDtypeStruct
     small = sds((rows, heads), F32)
     padded = -(-rows // 8) * 8
@@ -418,39 +401,37 @@
             pltpu.VMEM((rows, heads), F32),
             pltpu.VMEM((1, width), F32),
             pltpu.VMEM(vg_shape, BF16),
-            pltpu.VMEM((2 * cq, width), BF16),
+            pltpu.VMEM((4 * cq, width), BF16),
             pltpu.VMEM((2, heads, width), BF16),
             pltpu.VMEM((1, heads), F32),
             pltpu.VMEM((1, width), F32),
-            pltpu.VMEM(wo.shape, BF16),
+            pltpu.VMEM(o_shape, BF16),
             pltpu.VMEM((1, width), F32),
             pltpu.VMEM(routed_experts.shape, jnp.int32),
             pltpu.VMEM(route_weights.shape, F32),
             pltpu.VMEM((2, width, hidden), BF16),
             pltpu.VMEM((hidden, width), BF16),
-            pltpu.VMEM((n, rows, width), BF16),
-            pltpu.VMEM((names_width, n * rows), F32),
-            pltpu.VMEM((n, wanted, n * rows), BF16),
-            pltpu.VMEM((n * rows, columns), F32),
-            pltpu.VMEM((n, rows, total_cols), BF16),
-            pltpu.VMEM((n, rows, total_cols), BF16),
+            pltpu.VMEM((n // 2, rows, width), BF16),
+            pltpu.VMEM((names_width, n // 2 * rows), F32),
+            pltpu.VMEM((n, wanted, n // 2 * rows), BF16),
+            pltpu.VMEM((n // 2 * rows, 2 * columns), F32),
+            pltpu.VMEM((n // 2, 2, rows, total_cols), BF16),
+            pltpu.VMEM((n // 2, 2, rows, total_cols), BF16),
             pltpu.VMEM((heads, key_size, padded), F32),
             pltpu.VMEM((heads, rows, value_size), F32),
             pltpu.VMEM((heads, rows, value_size), F32),
             pltpu.VMEM((heads, rows, value_size), F32),
-            pltpu.VMEM((heads, n, rows, value_size), BF16),
-            pltpu.VMEM((n * wanted, columns), BF16),
-            pltpu.VMEM((n, wanted, columns), BF16),
-            pltpu.VMEM((n, rows, columns), BF16),
-            pltpu.VMEM((n, rows, columns), BF16),
+            pltpu.VMEM((heads, n // 2, rows, value_size), BF16),
+            pltpu.VMEM((n * wanted, 2 * columns), BF16),
+            pltpu.VMEM((n, wanted, 2 * columns), BF16),
+            pltpu.VMEM((n // 2, rows, 2 * columns), BF16),
+            pltpu.VMEM((n // 2, rows, 2 * columns), BF16),
             pltpu.VMEM((n, SLOTS, width), BF16),
             pltpu.SemaphoreType.DMA((15,)),
-            pltpu.SemaphoreType.DMA((5 + heads,)),
-            pltpu.SemaphoreType.DMA((heads, n // 2 - 1)),
-            pltpu.SemaphoreType.DMA((heads + 1,)),
+            pltpu.SemaphoreType.DMA((8 + heads,)),
             pltpu.SemaphoreType.DMA((heads,)),
             pltpu.SemaphoreType.DMA((heads,)),
-            pltpu.SemaphoreType.DMA((3,)),
+            pltpu.SemaphoreType.DMA((7,)),
         ],
         compiler_params=pltpu.CompilerParams(
             collective_id=0, has_side_effects=True, vmem_limit_bytes=40 << 20

time: 37.5 us -> 36.5 us (0.973)
  Pallas kernels: 36.6 us -> 35.6 us
    pallas_call x1, Pallas kernels: 33.4 us -> 32.3 us  [body(): pl.pallas_call(functools.partial(layer_kernel, n, heads, key_size, value_...]
where the time goes in v4:
time: 36.5 us; the launch traced here: 36.2 us
  Pallas kernels  35.6 us (98%)
  between operations  0.65 us (2%)
    pallas_call x1, Pallas kernels, body(): pl.pallas_call(functools.partial(layer_kernel, n, heads, key_size, value_...  32.3 us
    pallas_call x1, Pallas kernels, body(): pl.pallas_call(combine_kernel, out_shape=(sds((rows, width), BF16), sds(m...  3.26 us

profile of v4, /device:TPU:0, one launch (start us, length us, event | category | flops | bytes accessed | tf_op | source)
XLA Modules:
  0.0 36.2 jit_solution(2056099740036769875)
XLA Ops:
  0.6 32.3 %layer.1 = (f32[4,4,256,512]{3,2,1,0:T(8,128)S(1)}, bf16[16,2,2048]{2,1,0:T(2,128)(2,1)S(1)}, f32[4,2048]{1,0:T(4,128)S(1)}, f32[4,128]{1,0:T(4,128)S(1)}, f32[4,4]{1,0:T(4,128)S(1)}) custom-call(bf16[4,2048]{1,0:T(4,128)(2,1)} %tokens.1, f32[4,4,256,512]{3,2,1,0:T(8,128)} %memory.1, f32[4,4]{1,0:T(4,128)} %max_state.1, f32[1,2048]{1,0:T(1,128)} %bitcast.12, ...), custom_call_target="tpu_custom_call" | custom-call | tf_op jit(solution)/shard_map/layer/pallas_call | solution.py:388
  33.0 3.3 %combine.1 = (bf16[4,2048]{1,0:T(4,128)(2,1)}, f32[4,4,256,512]{3,2,1,0:T(8,128)}, f32[4,4]{1,0:T(4,128)}) custom-call(f32[4,4,256,512]{3,2,1,0:T(8,128)S(1)} %get-tuple-element.8.memory, bf16[16,2,2048]{2,1,0:T(2,128)(2,1)S(1)} %get-tuple-element.9.results, f32[4,2048]{1,0:T(4,128)S(1)} %get-tuple-element.10.residual, ...), custom_call_target="tpu_custom_call" | custom-call | tf_op jit(solution)/shard_map/combine/pallas_call | solution.py:449

commit v5 on v4

--- a/solution.py
+++ b/solution.py
@@ -83,7 +83,7 @@
     new_memory, results, residual_out, picks_out, max_out,
     tok_s, max_s, ngain_s, vg_w, qk_w, gates_w, bias_s,
     hgain_s, o_w, egain_s, routed_s, rw_s, up_w, down_w,
-    all_s, names_s, pick_s, x_s, proj_s, back_s, kt_s, v_s, c_s, w_s, mix_s,
+    all_s, lhs_s, turned_w, names_s, pick_s, x_s, proj_s, back_s, kt_s, v_s, c_s, w_s, mix_s,
     res_s, needed_s, own_s, owned_s, out_s,
     local_sem, send_sem, column_sem, part_sem, group_sem,
 ):
@@ -142,8 +142,7 @@
         taken = taken + named[r : r + 1]
     chosen = jnp.concatenate(chosen, axis=0)
     for t in range(n // 2):
-        for c in range(2):
-            proj_s[t, c, :, :names_width] = chosen.astype(BF16)
+        proj_s[t, :, :names_width] = chosen.astype(BF16)
     picks_out[...] = chosen * weighed
 
     gain = ngain_s[...]
@@ -158,7 +157,10 @@
     written = jnp.exp(input_logit - new_max) * key_size**-0.5
 
     pl.semaphore_wait(barrier, n - 1)
-    spread(n, me, lambda mask: tok_s, all_s.at[chip], send_sem.at[0], lambda mask: group_sem.at[0])
+    spread(
+        n, me, lambda mask: tok_s, all_s.at[chip], send_sem.at[0],
+        lambda mask: group_sem.at[0 if mask < n // 2 else 7],
+    )
     all_s[chip] = tok_s[...]
     partner = flip(me, 1)
     for i, block in enumerate(shared):
@@ -167,14 +169,25 @@
     per = n // heads
     arrived(shared[0], group_sem.at[3])
     arrived(shared[1], group_sem.at[4])
-    arrived(all_s.at[same], group_sem.at[0])
-    entries = jnp.concatenate([all_s[t].astype(F32) for t in range(n // 2)], axis=0)
-    entries = scaled_norm(entries, gain).astype(BF16)
-    for table, start, size in ((vg_w, names_width, 2 * cv), (qk_w, names_width + 2 * cv, 2 * cq)):
-        made = apply(entries, table[...]).astype(BF16).astype(F32)
+    turned_w[...] = qk_w[...].T
+
+    def prepare(half):
+        count = n // 4
+        at = pl.ds(pl.multiple_of(half * count * rows, count * rows), count * rows)
+        entries = [all_s[half * count + t].astype(F32) for t in range(count)]
+        lhs_s[at, :] = scaled_norm(jnp.concatenate(entries, axis=0), gain).astype(BF16)
+
+    half = lax.div(chip, n // 4)
+    arrived(all_s.at[pl.ds(0, n // 4 - 1)], group_sem.at[0])
+    prepare(half)
+    arrived(all_s.at[pl.ds(0, n // 4)], group_sem.at[7])
+    prepare(1 - half)
+    gate_size = 2 * cv + 2 * cq
+    for table, start, size in ((vg_w, names_width, 2 * cv), (turned_w, names_width + 2 * cv, 2 * cq)):
+        made = apply(lhs_s[...], table[...]).astype(BF16).astype(F32)
         for t in range(n // 2):
             for c in range(2):
-                proj_s[t, c, :, start : start + size] = (
+                proj_s[t, :, start + c * gate_size : start + c * gate_size + size] = (
                     made[t * rows : (t + 1) * rows, c * size : (c + 1) * size].astype(BF16)
                 )
     spread(
@@ -197,7 +210,10 @@
 
     def read(h):
         pieces = [
-            back_s[h * (per // 2) + t // 2, t % 2][:, names_width:].astype(F32) for t in range(per)
+            back_s[h * (per // 2) + t // 2][
+                :, names_width + t % 2 * gate_size : names_width + (t % 2 + 1) * gate_size
+            ].astype(F32)
+            for t in range(per)
         ]
         v = jnp.concatenate([b[:, :cv] for b in pieces], axis=1)
         g = jnp.concatenate([b[:, cv : 2 * cv] for b in pieces], axis=1)
@@ -229,7 +245,7 @@
         mine = mix_s.at[h, chip]
         spread(n, me, lambda mask: mine, mine, send_sem.at[2], lambda mask: group_sem.at[6])
     names_s[...] = jnp.concatenate(
-        [back_s[t, 0][:, :names_width].astype(F32) for t in range(n // 2)], axis=0
+        [back_s[t][:, :names_width].astype(F32) for t in range(n // 2)], axis=0
     ).T
     wanted = SLOTS * n // 2
     place = lax.broadcasted_iota(jnp.int32, (wanted, n // 2 * rows), 0)
@@ -380,7 +396,7 @@
     vg_shape = (width, 4 * cv) if cv % 128 == 0 else (4 * cv, width)
     o_shape = (width, 2 * columns) if columns % 128 == 0 else (2 * columns, width)
     names_width = -(-SLOTS * n // 128) * 128
-    total_cols = names_width + 2 * cq + 2 * cv
+    total_cols = names_width + 4 * cq + 4 * cv
     wanted = SLOTS * n // 2
     sds = jax.ShapeDtypeStruct
     small = sds((rows, heads), F32)
@@ -412,11 +428,13 @@
             pltpu.VMEM((2, width, hidden), BF16),
             pltpu.VMEM((hidden, width), BF16),
             pltpu.VMEM((n // 2, rows, width), BF16),
+            pltpu.VMEM((n // 2 * rows, width), BF16),
+            pltpu.VMEM((width, 4 * cq), BF16),
             pltpu.VMEM((names_width, n // 2 * rows), F32),
             pltpu.VMEM((n, wanted, n // 2 * rows), BF16),
             pltpu.VMEM((n // 2 * rows, 2 * columns), F32),
-            pltpu.VMEM((n // 2, 2, rows, total_cols), BF16),
-            pltpu.VMEM((n // 2, 2, rows, total_cols), BF16),
+            pltpu.VMEM((n // 2, rows, total_cols), BF16),
+            pltpu.VMEM((n // 2, rows, total_cols), BF16),
             pltpu.VMEM((heads, key_size, padded), F32),
             pltpu.VMEM((heads, rows, value_size), F32),
             pltpu.VMEM((heads, rows, value_size), F32),
@@ -431,7 +449,7 @@
             pltpu.SemaphoreType.DMA((8 + heads,)),
             pltpu.SemaphoreType.DMA((heads,)),
             pltpu.SemaphoreType.DMA((heads,)),
-            pltpu.SemaphoreType.DMA((7,)),
+            pltpu.SemaphoreType.DMA((8,)),
         ],
         compiler_params=pltpu.CompilerParams(
             collective_id=0, has_side_effects=True, vmem_limit_bytes=40 << 20

time: 36.5 us -> 36 us (0.986)
  Pallas kernels: 35.6 us -> 35.1 us
    pallas_call x1, Pallas kernels: 32.3 us -> 31.8 us  [body(): pl.pallas_call(functools.partial(layer_kernel, n, heads, key_size, value_...]
where the time goes in v5:
time: 36 us; the launch traced here: 35.7 us
  Pallas kernels  35.1 us (98%)
  between operations  0.65 us (2%)
    pallas_call x1, Pallas kernels, body(): pl.pallas_call(functools.partial(layer_kernel, n, heads, key_size, value_...  31.8 us
    pallas_call x1, Pallas kernels, body(): pl.pallas_call(combine_kernel, out_shape=(sds((rows, width), BF16), sds(m...  3.26 us

profile of v5, /device:TPU:0, one launch (start us, length us, event | category | flops | bytes accessed | tf_op | source)
XLA Modules:
  0.0 35.7 jit_solution(7408894587099764064)
XLA Ops:
  0.6 31.8 %layer.1 = (f32[4,4,256,512]{3,2,1,0:T(8,128)S(1)}, bf16[16,2,2048]{2,1,0:T(2,128)(2,1)S(1)}, f32[4,2048]{1,0:T(4,128)S(1)}, f32[4,128]{1,0:T(4,128)S(1)}, f32[4,4]{1,0:T(4,128)S(1)}) custom-call(bf16[4,2048]{1,0:T(4,128)(2,1)} %tokens.1, f32[4,4,256,512]{3,2,1,0:T(8,128)} %memory.1, f32[4,4]{1,0:T(4,128)} %max_state.1, f32[1,2048]{1,0:T(1,128)} %bitcast.12, ...), custom_call_target="tpu_custom_call" | custom-call | tf_op jit(solution)/shard_map/layer/pallas_call | solution.py:404
  32.4 3.3 %combine.1 = (bf16[4,2048]{1,0:T(4,128)(2,1)}, f32[4,4,256,512]{3,2,1,0:T(8,128)}, f32[4,4]{1,0:T(4,128)}) custom-call(f32[4,4,256,512]{3,2,1,0:T(8,128)S(1)} %get-tuple-element.8.memory, bf16[16,2,2048]{2,1,0:T(2,128)(2,1)S(1)} %get-tuple-element.9.results, f32[4,2048]{1,0:T(4,128)S(1)} %get-tuple-element.10.residual, ...), custom_call_target="tpu_custom_call" | custom-call | tf_op jit(solution)/shard_map/combine/pallas_call | solution.py:467
